TPU v7x, 32 devices: a whole 2x2x4 slice. The times are simulated.
32 devices in a mesh: sp: 8 (over z, y), tp: 4 (over x, core).
Axes of the slice: x: 2, y: 2, z: 4, core: 2. Of those that a mesh axis runs over, the one named last changes fastest.
Arguments:
- tokens: bfloat16 [4096, 2048], P(('sp', 'tp')), may hold values from -6 to 6
- norm_gain: float32 [2048], replicated, may hold values from 0.25 to 5
- w_query_one: bfloat16 [2048, 512], P(None, 'tp'), may hold values from -0.21875 to 0.21875
- w_query_two: bfloat16 [2048, 512], P(None, 'tp'), may hold values from -0.21875 to 0.21875
- w_key_one: bfloat16 [2048, 512], P(None, 'tp'), may hold values from -0.125 to 0.125
- w_key_two: bfloat16 [2048, 512], P(None, 'tp'), may hold values from -0.125 to 0.125
- w_value: bfloat16 [2048, 1024], P(None, 'tp'), may hold values from -0.125 to 0.125
- mix_lambda: float32 [8], P('tp'), may hold values from 0.3 to 0.8
- head_gain: float32 [128], replicated, may hold values from 0.1 to 1.9
- w_ret_query: bfloat16 [2048, 512], P(None, 'tp'), may hold values from -0.125 to 0.125
- w_ret_key: bfloat16 [2048, 512], P(None, 'tp'), may hold values from -0.125 to 0.125
- w_ret_value: bfloat16 [2048, 1024], P(None, 'tp'), may hold values from -0.125 to 0.125
- retain_log: float32 [8, 4096], P('tp', 'sp'), may hold values from -1 to 0
- init_state: float32 [8, 64, 128], P('tp'), may hold values from -144 to 144
- w_out_diff: bfloat16 [1024, 2048], P('tp'), may hold values from -0.125 to 0.125
- w_out_ret: bfloat16 [1024, 2048], P('tp'), may hold values from -0.125 to 0.125
Outputs:
- mixed: bfloat16 [4096, 2048], P(('sp', 'tp'))
All inputs are finite; a program needn't handle non-finite values.
Results may differ from a plain program's by a relative error of at most 0.015.
The roundings to bfloat16 on the way count: a program that leaves them out, or rounds other values in their place, can miss the bound.
Values may be sent and summed in bfloat16 or wider, within the bound.
A program may use at most 128 MiB of HBM per device.

v0:
```python
import functools

import jax
import jax.numpy as jnp
from jax import lax
from jax.experimental import pallas as pl
from jax.experimental.pallas import tpu as pltpu
from jax.sharding import PartitionSpec as P

BLOCK = 256
NORM_EPS = 1e-06
HEAD_EPS = 1e-05
DIFF_SCALE = 0.8
HIGHEST = lax.Precision.HIGHEST
MESH = pl.DeviceIdType.MESH
F32 = jnp.float32
BF16 = jnp.bfloat16
VMEM_LIMIT = 60 * 1024 * 1024


def remote(src, dst, send, recv, where):
    return pltpu.make_async_remote_copy(
        src_ref=src, dst_ref=dst, send_sem=send, recv_sem=recv,
        device_id=where, device_id_type=MESH,
    )


def head_norm(values):
    return values * lax.rsqrt(jnp.mean(values * values, axis=-1, keepdims=True) + HEAD_EPS)


def nn(a, b, **kw):
    return lax.dot_general(a, b, (((1,), (0,)), ((), ())), preferred_element_type=F32, **kw)


def nt(a, b):
    return lax.dot_general(a, b, (((1,), (1,)), ((), ())), preferred_element_type=F32)


def tn(a, b):
    return lax.dot_general(a, b, (((0,), (0,)), ((), ())), preferred_element_type=F32)


def layer_kernel(nsp, ntp, widths, heads, rheads, lam_ref, tokens_ref, ngain_ref, gain_ref, log_ref,
                 init_ref, *refs):
    nw = len(widths)
    w_refs = refs[:nw]
    wd_ref, wr_ref, out_ref = refs[nw : nw + 3]
    (gat, wbuf, wobuf, kvs, sts, rbuf, qs, peak, den, acc, rmid, upd, mix, mine, sent, from_pair,
     from_chip, wsem, pair_send, cross_send, grecv, sem_z, sem_y, sem_rk, sem_zs, sem_ys, sem_rs,
     mpair_send, mpair_recv, mchip_send, mchip_recv) = refs[nw + 3 :]
    me = lax.axis_index("sp")
    b = lax.rem(me, 2)
    p = me // 2
    npair = nsp // 2
    up = {"sp": lax.rem(me + 2, nsp)}
    side = {"sp": me + 1 - 2 * b}
    tme = lax.axis_index("tp")
    core = lax.rem(tme, 2)
    chip = tme // 2
    nchip = ntp // 2
    tpair = tme + 1 - 2 * core
    pair = {"tp": tpair}
    own_rows = tokens_ref.shape[0]
    rows = own_rows * ntp
    chunk = rows // nchip
    kw = widths[2]
    hd = kw // heads
    val = gain_ref.shape[1]
    first_up = p < npair - 1

    barrier = pltpu.get_barrier_semaphore()

    def greet(where):
        pl.semaphore_signal(barrier, inc=1, device_id=where, device_id_type=MESH)

    greet(side)

    @pl.when(p > 0)
    def _():
        greet({"sp": lax.rem(me + nsp - 2, nsp)})

    @pl.when(first_up)
    def _():
        greet(up)

    greet(pair)
    for d in range(1, nchip):
        greet({"tp": lax.rem(chip + d, nchip) * 2 + core})

    order = (2, 3, 4, 0, 1, 5, 6, 7)
    starts = [sum(widths[:n]) for n in range(nw)]
    loads = {}
    for n in order:
        at = starts[n]
        loads[n] = pltpu.make_async_copy(w_refs[n], wbuf.at[:, at : at + widths[n]], wsem.at[n])
        loads[n].start()
    depth = wd_ref.shape[0]
    out_loads = [
        pltpu.make_async_copy(wd_ref, wobuf.at[:depth], wsem.at[nw]),
        pltpu.make_async_copy(wr_ref, wobuf.at[depth:], wsem.at[nw + 1]),
    ]
    for load in out_loads:
        load.start()
    floats = tokens_ref[...].astype(F32)
    gat[tme] = (
        floats * lax.rsqrt(jnp.mean(floats * floats, axis=-1, keepdims=True) + NORM_EPS) * ngain_ref[...]
    ).astype(BF16)
    pl.semaphore_wait(
        barrier, 1 + nchip + jnp.minimum(p, 1) + jnp.minimum(npair - 1 - p, 1)
    )
    copies = []

    def slab(which, half):
        return gat.at[which, pl.ds(half * (own_rows // 2), own_rows // 2)]

    for d in range(1, nchip):
        there = {"tp": lax.rem(chip + d, nchip) * 2 + core}
        for half in range(2):
            copies.append(remote(slab(tme, half), slab(tme, half), cross_send.at[d, half],
                                 grecv.at[tme, half], there))
            copies[-1].start()

    def to_pair(which, half):
        copies.append(remote(slab(which, half), slab(which, half), pair_send.at[which // 2, half],
                             grecv.at[which, half], pair))
        copies[-1].start()

    def landed(which, half):
        remote(slab(which, half), slab(which, half), pair_send.at[which // 2, half],
               grecv.at[which, half], pair).wait_recv()

    def keys_at(d):
        which = lax.rem(chip + nchip - d, nchip)
        return pl.ds(pl.multiple_of(which * chunk, chunk), chunk)

    def kv_copy(i, j, d, sem, where):
        piece = kvs.at[j, keys_at(d)]
        return remote(piece, piece, sem.at[i, d], sem_rk.at[j, d], where)

    def st_copy(i, j, sem, where):
        return remote(sts.at[j], sts.at[j], sem.at[i], sem_rs.at[j], where)

    qlane = lax.broadcasted_iota(jnp.int32, (chunk, kw), 1)

    def project(d):
        which = lax.rem(chip + nchip - d, nchip)
        both = gat[pl.ds(which * 2, 2)].reshape(chunk, gat.shape[2])
        at = keys_at(d)

        def run(lo, hi, put):
            if d == 0:
                for n in range(lo, hi):
                    loads[n].wait()
            span = sum(widths[lo:hi])
            cut = 256 if span % 256 == 0 else span
            for c in range(0, span, cut):
                put(c, cut, nn(both, wbuf[:, starts[lo] + c : starts[lo] + c + cut]).astype(BF16))

        def put_kv(c, cut, value):
            kvs[me, at, c : c + cut] = value

        def put_r(c, cut, value):
            rbuf[at, c : c + cut] = value

        run(2, 5, put_kv)
        for m in range(2):
            if d == 0:
                loads[m].wait()
            piece = nn(both, wbuf[:, starts[m] : starts[m] + kw]).astype(BF16).astype(F32) * hd ** (-0.5)
            for h in range(heads):
                keep = (qlane >= h * hd) & (qlane < (h + 1) * hd)
                qs[m * heads + h, at, :] = jnp.where(keep, piece, 0.0).astype(BF16)

        @pl.when(first_up)
        def _():
            kv_copy(0, me, d, sem_z, up).start()

        @pl.when(b == 0)
        def _():
            kv_copy(0, me, d, sem_y, side).start()

        run(5, 8, put_r)

    def forward(i, d):
        jz = 2 * (p - i) + b

        @pl.when(i <= p)
        def _():
            kv_copy(i, jz, d, sem_z, up).wait_recv()

            @pl.when(first_up)
            def _():
                kv_copy(i, jz, d, sem_z, up).start()

            kv_copy(i, jz, d, sem_y, side).start()

    for half in range(2):
        to_pair(tme, half)
    for half in range(2):
        landed(tpair, half)
    project(0)
    peak[...] = jnp.full(peak.shape, -jnp.inf, F32)
    den[...] = jnp.zeros(den.shape, F32)
    acc[...] = jnp.zeros(acc.shape, F32)
    forward(1, 0)
    for d in range(1, nchip):
        other = lax.rem(chip + nchip - d, nchip)
        for half in range(2):
            landed(other * 2 + core, half)
            to_pair(other * 2 + core, half)
        for half in range(2):
            landed(other * 2 + 1 - core, half)
        project(d)
    if npair > 1:
        forward(2, 0)

    blk = BLOCK
    nblk = rows // blk
    rkw = rheads * hd
    tt = lax.broadcasted_iota(jnp.int32, (blk, blk), 0)
    uu = lax.broadcasted_iota(jnp.int32, (blk, blk), 1)
    lane = lax.broadcasted_iota(jnp.int32, (blk, rkw), 1)
    srow = lax.broadcasted_iota(jnp.int32, (rkw, val), 0)
    decays = []
    span_state = jnp.zeros((rkw, val), F32)
    span_logs = []
    for h in range(rheads):
        ours = (lane >= h * hd) & (lane < (h + 1) * hd)
        keep = (srow >= h * hd) & (srow < (h + 1) * hd)
        state = jnp.zeros((rkw, val), F32)
        log_all = jnp.zeros((1, 1), F32)
        for n in range(nblk):
            at = slice(n * blk, (n + 1) * blk)
            row = log_ref[h : h + 1, at]
            full = jnp.broadcast_to(row, (blk, blk))
            c_col = jnp.sum(jnp.where(uu <= tt, full, 0.0), axis=1, keepdims=True)
            l_col = jnp.sum(jnp.where(uu == tt, full, 0.0), axis=1, keepdims=True)
            c_row = jnp.sum(jnp.where(tt <= uu, l_col, 0.0), axis=0, keepdims=True)
            last = c_col[blk - 1 : blk, :]
            query = jnp.where(ours, rbuf[at, :rkw].astype(F32), 0.0)
            keys = rbuf[at, rkw : 2 * rkw]
            values = rbuf[at, 2 * rkw + h * val : 2 * rkw + (h + 1) * val]
            raw = nt(query.astype(BF16), keys)
            gap = jnp.where(uu <= tt, c_col - c_row, -jnp.inf)
            g = (raw * hd ** (-0.5) * jnp.exp(gap)).astype(BF16)
            rmid[h, at, :] = nn(g, values)
            kd = (keys.astype(F32) * hd ** (-0.5) * jnp.exp(last - c_col)).astype(BF16)
            new = jnp.where(keep, tn(kd, values), 0.0)
            upd[h, n] = new
            state = jnp.exp(last) * state + new
            log_all = log_all + last
            decays.append((c_col, last))
        span_state = span_state + state
        span_logs.append(log_all)
    sts[me, :rkw, :] = span_state.astype(BF16)
    for h in range(rheads):
        wide = jnp.broadcast_to(span_logs[h], (16, val))
        hi = wide.astype(BF16)
        sts[me, rkw + 32 * h : rkw + 32 * h + 16, :] = hi
        sts[me, rkw + 32 * h + 16 : rkw + 32 * h + 32, :] = (wide - hi.astype(F32)).astype(BF16)

    qb = min(rows, 256)

    def attend(j, diagonal):

        @pl.loop(0, 2 * heads)
        def _(mh):
            m = mh // heads
            h = lax.rem(mh, heads)
            kcol = pl.ds(pl.multiple_of(m * kw, kw), kw)
            vcol = pl.ds(pl.multiple_of(2 * kw + h * val, val), val)
            for n in range(rows // qb):
                at = slice(n * qb, (n + 1) * qb)
                count = (n + 1) * qb if diagonal else rows
                krows = slice(0, count)
                scores = nt(qs[mh, at, :], kvs[j, krows, kcol])
                if diagonal:
                    ti = lax.broadcasted_iota(jnp.int32, (qb, count), 0) + n * qb
                    ui = lax.broadcasted_iota(jnp.int32, (qb, count), 1)
                    scores = jnp.where(ui <= ti, scores, -jnp.inf)
                old = peak[mh, at, :]
                top = jnp.maximum(old, jnp.max(scores, axis=1, keepdims=True))
                e = jnp.exp(scores - top[:, :1])
                part = e[:, :128]
                for c in range(128, count, 128):
                    part = part + e[:, c : c + 128]
                weighted = nn(e.astype(BF16), kvs[j, krows, vcol])
                rescale = jnp.exp(old - top)
                peak[mh, at, :] = top
                den[mh, at, :] = den[mh, at, :] * rescale + part
                acc[mh, at, :] = acc[mh, at, :] * rescale[:, :1] + weighted

    @pl.loop(3, npair + 1)
    def _(i):
        forward(i, 0)

    attend(me, True)

    @pl.when(first_up)
    def _():
        st_copy(0, me, sem_zs, up).start()

    @pl.when(b == 0)
    def _():
        st_copy(0, me, sem_ys, side).start()

    @pl.loop(1, npair + 1)
    def _(i):
        jz = 2 * (p - i) + b
        jy = 2 * (p - i + 1) + 1 - b
        for d in range(1, nchip):
            forward(i, d)

        @pl.when(i <= p)
        def _():
            st_copy(i, jz, sem_zs, up).wait_recv()

            @pl.when(first_up)
            def _():
                st_copy(i, jz, sem_zs, up).start()

            st_copy(i, jz, sem_ys, side).start()
            attend(jz, False)

        @pl.when((i - 1 <= p) & ((b == 1) | (i > 1)))
        def _():
            for d in range(nchip):
                kv_copy(i, jy, d, sem_y, side).wait_recv()
            st_copy(i, jy, sem_ys, side).wait_recv()
            attend(jy, False)

    first = []
    for h in range(rheads):
        parts = [jnp.zeros((hd, val), F32)] * h + [init_ref[h]] + [jnp.zeros((hd, val), F32)] * (rheads - 1 - h)
        first.append(jnp.concatenate(parts, axis=0) if rheads > 1 else parts[0])

    def join(j, states):
        out = []
        for h in range(rheads):
            keep = (srow >= h * hd) & (srow < (h + 1) * hd)
            base = rkw + 32 * h
            log = sts[j, base : base + 16, :].astype(F32) + sts[j, base + 16 : base + 32, :].astype(F32)
            piece = jnp.where(keep, sts[j, :rkw, :].astype(F32), 0.0)
            out.append(jnp.exp(log[:1, :]) * states[h] + piece)
        return tuple(out)

    carried = lax.fori_loop(0, me, join, tuple(first))
    for h in range(rheads):
        state = carried[h]
        for n in range(nblk):
            at = slice(n * blk, (n + 1) * blk)
            c_col, last = decays[h * nblk + n]
            query = rbuf[at, :rkw].astype(F32) * jnp.exp(c_col)
            result = rmid[h, at, :] + nn(query, state, precision=HIGHEST)
            if n + 1 < nblk:
                state = jnp.exp(last) * state + upd[h, n]
            mix[at, heads * val + h * val : heads * val + (h + 1) * val] = head_norm(result).astype(BF16)
    for h in range(heads):
        pieces = []
        for m in range(2):
            mh = m * heads + h
            total = jnp.sum(den[mh], axis=1, keepdims=True)
            pieces.append(acc[mh] / total)
        mixed = pieces[0] - lam_ref[h] * pieces[1]
        mix[:, h * val : (h + 1) * val] = (head_norm(mixed) * gain_ref[...] * DIFF_SCALE).astype(BF16)
    for load in out_loads:
        load.wait()

    width = out_ref.shape[1]
    cut = mine.shape[2]
    npiece = width // cut

    def partial(owner, n):
        part = mix[pl.ds(pl.multiple_of(owner * own_rows, own_rows), own_rows), :]
        return nn(part, wobuf[:, n * cut : (n + 1) * cut])

    def pair_copy(d, n):
        return remote(mine.at[d * npiece + n], from_pair.at[d * npiece + n], mpair_send.at[d, n],
                      mpair_recv.at[d, n], pair)

    def chip_copy(d, n):
        there = lax.rem(chip + d, nchip) * 2 + core
        return remote(sent.at[d * npiece + n], from_chip.at[d * npiece + n], mchip_send.at[d, n],
                      mchip_recv.at[d, n], {"tp": there})

    targets = list(range(1, nchip)) + [0]
    for d in targets:
        target = lax.rem(chip + d, nchip) * 2
        for n in range(npiece):
            mine[d * npiece + n] = partial(target + 1 - core, n).astype(BF16)
            pair_copy(d, n).start()
        if d:
            for n in range(npiece):
                ours = partial(target + core, n)
                pair_copy(d, n).wait_recv()
                sent[d * npiece + n] = (ours + from_pair[d * npiece + n].astype(F32)).astype(BF16)
                chip_copy(d, n).start()
    for n in range(npiece):
        total = partial(tme, n)
        pair_copy(0, n).wait_recv()
        total = total + from_pair[n].astype(F32)
        for d in range(1, nchip):
            chip_copy(d, n).wait_recv()
            total = total + from_chip[d * npiece + n].astype(F32)
        out_ref[:, n * cut : (n + 1) * cut] = total.astype(BF16)

    for copy in copies:
        copy.wait_send()

    @pl.loop(0, npair)
    def _(i):
        j = 2 * (p - i) + b

        @pl.when((i <= p) & first_up)
        def _():
            for d in range(nchip):
                kv_copy(i, j, d, sem_z, up).wait_send()
            st_copy(i, j, sem_zs, up).wait_send()

        @pl.when((i <= p) & ((i > 0) | (b == 0)))
        def _():
            for d in range(nchip):
                kv_copy(i, j, d, sem_y, side).wait_send()
            st_copy(i, j, sem_ys, side).wait_send()

    for d in targets:
        for n in range(npiece):
            pair_copy(d, n).wait_send()
            if d:
                chip_copy(d, n).wait_send()


VMEM = pl.BlockSpec(memory_space=pltpu.VMEM)
ANY = pl.BlockSpec(memory_space=pl.ANY)
SMEM = pl.BlockSpec(memory_space=pltpu.SMEM)
DMA = pltpu.SemaphoreType.DMA


def params(number):
    return pltpu.CompilerParams(
        collective_id=number, has_side_effects=True, vmem_limit_bytes=VMEM_LIMIT
    )


def on_device(nsp, ntp, tokens, norm_gain, w_query_one, w_query_two, w_key_one, w_key_two, w_value,
              mix_lambda, head_gain, w_ret_query, w_ret_key, w_ret_value, retain_log, init_state,
              w_out_diff, w_out_ret):
    weights = (w_query_one, w_query_two, w_key_one, w_key_two, w_value, w_ret_query, w_ret_key, w_ret_value)
    widths = tuple(w.shape[1] for w in weights)
    own_rows, model = tokens.shape
    rows = own_rows * ntp
    nchip = ntp // 2
    npair = nsp // 2
    heads = mix_lambda.shape[0]
    rheads, hd, val = init_state.shape
    kw = widths[2]
    width = w_out_diff.shape[1]
    npiece = 4
    cut = width // npiece
    return pl.pallas_call(
        functools.partial(layer_kernel, nsp, ntp, widths, heads, rheads),
        out_shape=jax.ShapeDtypeStruct((own_rows, width), BF16),
        in_specs=[SMEM] + [VMEM] * 5 + [ANY] * (len(weights) + 2),
        out_specs=VMEM,
        scratch_shapes=[
            pltpu.VMEM((ntp, own_rows, model), BF16),
            pltpu.VMEM((model, sum(widths)), BF16),
            pltpu.VMEM((w_out_diff.shape[0] + w_out_ret.shape[0], width), BF16),
            pltpu.VMEM((nsp, rows, sum(widths[2:5])), BF16),
            pltpu.VMEM((nsp, rheads * hd + 32 * rheads, val), BF16),
            pltpu.VMEM((rows, sum(widths[5:])), BF16),
            pltpu.VMEM((2 * heads, rows, kw), BF16),
            pltpu.VMEM((2 * heads, rows, 128), F32),
            pltpu.VMEM((2 * heads, rows, 128), F32),
            pltpu.VMEM((2 * heads, rows, val), F32),
            pltpu.VMEM((rheads, rows, val), F32),
            pltpu.VMEM((rheads, rows // BLOCK, rheads * hd, val), F32),
            pltpu.VMEM((rows, (heads + rheads) * val), BF16),
            pltpu.VMEM((nchip * npiece, own_rows, cut), BF16),
            pltpu.VMEM((nchip * npiece, own_rows, cut), BF16),
            pltpu.VMEM((nchip * npiece, own_rows, cut), BF16),
            pltpu.VMEM((nchip * npiece, own_rows, cut), BF16),
            DMA((len(weights) + 2,)),
            DMA((nchip, 2)),
            DMA((nchip, 2)),
            DMA((ntp, 2)),
            DMA((npair + 1, nchip)),
            DMA((npair + 1, nchip)),
            DMA((nsp, nchip)),
            DMA((npair + 1,)),
            DMA((npair + 1,)),
            DMA((nsp,)),
            DMA((nchip, npiece)),
            DMA((nchip, npiece)),
            DMA((nchip, npiece)),
            DMA((nchip, npiece)),
        ],
        compiler_params=params(0),
        name="layer",
    )(mix_lambda, tokens, norm_gain[None, :], head_gain[None, :], retain_log, init_state, *weights,
      w_out_diff, w_out_ret)


def solution(mesh):
    in_specs = (
        P(("sp", "tp"), None),
        P(),
        P(None, "tp"),
        P(None, "tp"),
        P(None, "tp"),
        P(None, "tp"),
        P(None, "tp"),
        P("tp"),
        P(),
        P(None, "tp"),
        P(None, "tp"),
        P(None, "tp"),
        P("tp", "sp"),
        P("tp", None, None),
        P("tp", None),
        P("tp", None),
    )
    body = functools.partial(on_device, mesh.shape["sp"], mesh.shape["tp"])
    return jax.shard_map(
        body, mesh=mesh, in_specs=in_specs, out_specs=P(("sp", "tp"), None), check_vma=False
    )
```

profile of v0, /device:TPU:29, one launch (start us, length us, event | category | flops | bytes accessed | tf_op | source)
XLA Modules:
  0.0 85.2 jit_solution(10773345378971208054)
XLA Ops:
  0.0 83.3 %layer.1 = bf16[128,2048]{1,0:T(8,128)(2,1)} custom-call(f32[2]{0:T(128)} %lam_ref.1, bf16[128,2048]{1,0:T(8,128)(2,1)} %tokens_ref.1, f32[1,2048]{1,0:T(1,128)} %bitcast.2, f32[1,128]{1,0:T(1,128)} %bitcast.3, f32[2,512]{1,0:T(2,128)} %log_ref.1, f32[2,64,128]{2,1,0:T(8,128)} %init_ref.1, bf16[2048,128]{1,0:T(8,128)(2,1)} %refs_0_.1, ...), custom_call_target="tpu_custom_call" | custom-call | tf_op jit(solution)/shard_map/layer/pallas_call | solution.py:461
  83.3 1.9 %copy.18 = bf16[128,2048]{1,0:T(8,128)(2,1)} copy(bf16[128,2048]{1,0:T(8,128)(2,1)} %layer.1) | data formatting | bytes 1048576
where the time goes:
time: 85.3 us; the launch traced here: 85.2 us
  Pallas kernels  83.3 us (98%)
  local copies, waits for them, and re-layouts  1.88 us (2%)
    pallas_call x1, Pallas kernels, on_device(): pl.pallas_call(functools.partial(layer_kernel, nsp, ntp, widths, heads, r...  83.3 us
    unnamed x1, local copies, waits for them, and re-layouts  1.88 us

commit v1 on v0

v1 whole, which is shorter than its diff:
```python
import functools

import jax
import jax.numpy as jnp
from jax import lax
from jax.experimental import pallas as pl
from jax.experimental.pallas import tpu as pltpu
from jax.sharding import PartitionSpec as P

BLOCK = 256
SQUARE = 4
NORM_EPS = 1e-06
HEAD_EPS = 1e-05
DIFF_SCALE = 0.8
HIGHEST = lax.Precision.HIGHEST
MESH = pl.DeviceIdType.MESH
F32 = jnp.float32
BF16 = jnp.bfloat16
VMEM_LIMIT = 60 * 1024 * 1024


def remote(src, dst, send, recv, where):
    return pltpu.make_async_remote_copy(
        src_ref=src, dst_ref=dst, send_sem=send, recv_sem=recv,
        device_id=where, device_id_type=MESH,
    )


def head_norm(values):
    return values * lax.rsqrt(jnp.mean(values * values, axis=-1, keepdims=True) + HEAD_EPS)


def nn(a, b, **kw):
    return lax.dot_general(a, b, (((1,), (0,)), ((), ())), preferred_element_type=F32, **kw)


def nt(a, b):
    return lax.dot_general(a, b, (((1,), (1,)), ((), ())), preferred_element_type=F32)


def tn(a, b):
    return lax.dot_general(a, b, (((0,), (0,)), ((), ())), preferred_element_type=F32)


def layer_kernel(nsp, ntp, widths, heads, rheads, lam_ref, tokens_ref, ngain_ref, gain_ref, log_ref,
                 init_ref, *refs):
    nw = len(widths)
    w_refs = refs[:nw]
    wd_ref, wr_ref, out_ref = refs[nw : nw + 3]
    (gat, wbuf, wobuf, sndq, sndkv, kvb, qraw, qs, lamv, peak, den, acc, dsend, dret, sts, rbuf, rmid,
     upd, mixr, mine, sent, from_pair, from_chip, wsem, lsem, pair_send, cross_send, grecv, sq_sem,
     skv_sem, inter_sem, fwd_sem, rq_sem, rkv_sem, ds_sem, rd_sem, sem_zs, sem_ys, sem_rs,
     mpair_send, mpair_recv, mchip_send, mchip_recv) = refs[nw + 3 :]
    me = lax.axis_index("sp")
    b = lax.rem(me, 2)
    p = me // 2
    npair = nsp // 2
    ngroup = nsp // SQUARE
    g = me // SQUARE
    s = lax.rem(me, SQUARE)
    up = {"sp": lax.rem(me + 2, nsp)}
    side = {"sp": me + 1 - 2 * b}
    tme = lax.axis_index("tp")
    core = lax.rem(tme, 2)
    chip = tme // 2
    nchip = ntp // 2
    tpair = tme + 1 - 2 * core
    pair = {"tp": tpair}
    own_rows = tokens_ref.shape[0]
    rows = own_rows * ntp
    chunk = rows // nchip
    kw = widths[2]
    hd = kw // heads
    val = gain_ref.shape[1]
    first_up = p < npair - 1

    held = (core, SQUARE - 1 - core)
    others = (1 - core, 2 + core)
    land = lax.rem((s + 1) // 2, 2)
    head_core = s // 2
    head_no = lax.rem(s, 2)
    base = SQUARE * g

    barrier = pltpu.get_barrier_semaphore()

    def greet(where):
        pl.semaphore_signal(barrier, inc=1, device_id=where, device_id_type=MESH)

    for k in range(1, ntp):
        greet({"tp": lax.rem(tme + k, ntp)})
    for k in range(1, SQUARE):
        for n in range(ntp):
            greet({"sp": base + lax.rem(s + k, SQUARE), "tp": n})
    for dg in range(1, ngroup):

        @pl.when(g + dg < ngroup)
        def _():
            for h in range(2):
                greet({"sp": base + SQUARE * dg + 2 * core + h, "tp": chip * 2 + land})

        @pl.when(g >= dg)
        def _():
            for t in range(2):
                greet({"sp": base - SQUARE * dg + held[t], "tp": chip * 2 + head_core})

    above = (s >= 2) & (g < ngroup - 1)
    below = (s < 2) & (g > 0)

    @pl.when(above)
    def _():
        greet(up)

    @pl.when(below)
    def _():
        greet({"sp": me - 2})

    order = (0, 1, 2, 3, 4, 5, 6, 7)
    starts = [sum(widths[:n]) for n in range(nw)]
    loads = {}
    for n in order:
        at = starts[n]
        loads[n] = pltpu.make_async_copy(w_refs[n], wbuf.at[:, at : at + widths[n]], wsem.at[n])
        loads[n].start()
    depth = wd_ref.shape[0]
    out_loads = [
        pltpu.make_async_copy(wd_ref, wobuf.at[:depth], wsem.at[nw]),
        pltpu.make_async_copy(wr_ref, wobuf.at[depth:], wsem.at[nw + 1]),
    ]
    for load in out_loads:
        load.start()
    floats = tokens_ref[...].astype(F32)
    gat[tme] = (
        floats * lax.rsqrt(jnp.mean(floats * floats, axis=-1, keepdims=True) + NORM_EPS) * ngain_ref[...]
    ).astype(BF16)
    for h in range(heads):
        lamv[core, 8 * h : 8 * h + 8, :] = jnp.full((8, 128), lam_ref[h], F32)
    pl.semaphore_wait(
        barrier,
        (ntp - 1) + (SQUARE - 1) * ntp + 2 * (ngroup - 1)
        + above.astype(jnp.int32) + below.astype(jnp.int32),
    )
    copies = []

    def begin(copy):
        copies.append(copy)
        copy.start()

    def slab(which, half):
        return gat.at[which, pl.ds(half * (own_rows // 2), own_rows // 2)]

    for d in range(1, nchip):
        there = {"tp": lax.rem(chip + d, nchip) * 2 + core}
        for half in range(2):
            begin(remote(slab(tme, half), slab(tme, half), cross_send.at[d, half],
                         grecv.at[tme, half], there))

    def to_pair(which, half):
        begin(remote(slab(which, half), slab(which, half), pair_send.at[which // 2, half],
                     grecv.at[which, half], pair))

    def landed(which, half):
        remote(slab(which, half), slab(which, half), pair_send.at[which // 2, half],
               grecv.at[which, half], pair).wait_recv()

    def lam_copy(who):
        return remote(lamv.at[who], lamv.at[who], lsem.at[0], lsem.at[1], pair)

    def part(d):
        return lax.rem(chip + nchip - d, nchip)

    def keys_at(d):
        return pl.ds(pl.multiple_of(part(d) * chunk, chunk), chunk)

    def q_copy(h, d):
        where = {"sp": base + 2 * core + h, "tp": chip * 2 + land}
        return remote(sndq.at[h, part(d)], qraw.at[s // 2, part(d)], sq_sem.at[h, d],
                      rq_sem.at[s // 2, d], where)

    def kv_copy(h, d, dg):
        where = {"sp": base + SQUARE * dg + 2 * core + h, "tp": chip * 2 + land}
        sem = skv_sem.at[h, d] if dg == 0 else inter_sem.at[dg - 1, h, d]
        return remote(sndkv.at[h, part(d)], kvb.at[me, part(d)], sem, rkv_sem.at[me, d], where)

    def q_local(h, d):
        return pltpu.make_async_copy(sndq.at[h, part(d)], qraw.at[s // 2, part(d)], rq_sem.at[s // 2, d])

    def kv_local(h, d):
        return pltpu.make_async_copy(sndkv.at[h, part(d)], kvb.at[me, part(d)], rkv_sem.at[me, d])

    def stays(h):
        return (2 * core + h == s) & (land == core)

    def fwd(span, t, dg, d):
        piece = kvb.at[span, part(d)]
        return remote(piece, piece, fwd_sem.at[dg, t, d], rkv_sem.at[span, d], pair)

    lane = lax.broadcasted_iota(jnp.int32, (chunk, 128), 1)

    def project(d):
        both = gat[pl.ds(part(d) * 2, 2)].reshape(chunk, gat.shape[2])

        def product(lo, hi):
            if d == 0:
                for n in range(lo, hi):
                    loads[n].wait()
            span = sum(widths[lo:hi])
            return nn(both, wbuf[:, starts[lo] : starts[lo] + span]).astype(BF16).astype(F32)

        def by_head(pairs):
            one, two = pairs[:, :kw], pairs[:, kw:]
            return (jnp.where(lane < hd, one, pltpu.roll(two, hd, 1)),
                    jnp.where(lane < hd, pltpu.roll(one, kw - hd, 1), two))

        queries = by_head(product(0, 2) * hd ** (-0.5))
        for h in range(heads):
            sndq[h, part(d)] = queries[h].astype(BF16)
        keys = by_head(product(2, 4))
        values = product(4, 5)
        for h in range(heads):
            sndkv[h, part(d), :chunk] = keys[h].astype(BF16)
            turned = values[:, h * val : (h + 1) * val].T.astype(BF16)
            for c in range(chunk // 128):
                at = chunk + c * val
                sndkv[h, part(d), at : at + val] = turned[:, c * 128 : (c + 1) * 128]
        for h in range(heads):

            @pl.when(stays(h))
            def _():
                q_local(h, d).start()
                kv_local(h, d).start()

            @pl.when(jnp.logical_not(stays(h)))
            def _():
                q_copy(h, d).start()
                kv_copy(h, d, 0).start()

        for dg in range(1, ngroup):

            @pl.when(g + dg < ngroup)
            def _():
                for h in range(heads):
                    kv_copy(h, d, dg).start()

    def project_ret(d):
        both = gat[pl.ds(part(d) * 2, 2)].reshape(chunk, gat.shape[2])
        if d == 0:
            for n in range(5, 8):
                loads[n].wait()
        span = sum(widths[5:8])
        for c in range(0, span, 256):
            rbuf[keys_at(d), c : c + 256] = nn(
                both, wbuf[:, starts[5] + c : starts[5] + c + 256]).astype(BF16)

    def st_copy(i, j, sem, where):
        return remote(sts.at[j], sts.at[j], sem.at[i], sem_rs.at[j], where)

    def relay(i):
        jz = 2 * (p - i) + b

        @pl.when(i <= p)
        def _():
            st_copy(i, jz, sem_zs, up).wait_recv()

            @pl.when(first_up)
            def _():
                st_copy(i, jz, sem_zs, up).start()

            st_copy(i, jz, sem_ys, side).start()

    for half in range(2):
        to_pair(tme, half)
    begin(lam_copy(core))
    peak[...] = jnp.full(peak.shape, -jnp.inf, F32)
    den[...] = jnp.zeros(den.shape, F32)
    acc[...] = jnp.zeros(acc.shape, F32)
    for half in range(2):
        landed(tpair, half)
    project(0)
    project_ret(0)

    def take(span, t, d, local):
        if local:
            here = (held[t] == s) & (head_core == core)

            @pl.when(here)
            def _():
                q_local(0, d).wait()
                kv_local(0, d).wait()

            @pl.when(jnp.logical_not(here))
            def _():
                remote(qraw.at[t, part(d)], qraw.at[t, part(d)], sq_sem.at[0, d],
                       rq_sem.at[t, d], pair).wait_recv()
                remote(kvb.at[span, part(d)], kvb.at[span, part(d)], skv_sem.at[0, d],
                       rkv_sem.at[span, d], pair).wait_recv()
        else:
            remote(kvb.at[span, part(d)], kvb.at[span, part(d)], skv_sem.at[0, d],
                   rkv_sem.at[span, d], pair).wait_recv()

    def ready(t, d):
        tile = t * nchip + part(d)
        value = qraw[t, part(d)].astype(F32)
        qs[tile, :chunk] = jnp.where(lane < hd, value, 0.0).astype(BF16)
        qs[tile, chunk:] = jnp.where(lane < hd, 0.0, value).astype(BF16)

    def needs(t):
        return (core == 1) | (t == 0)

    def take_own(d):
        for t in range(2):
            take(base + held[t], t, d, True)

            @pl.when(needs(t))
            def _():
                fwd(base + held[t], t, 0, d).start()

        for t in range(2):
            ready(t, d)

    def take_own_pair(d):
        for t in range(2):

            @pl.when((core == 0) | (t == 0))
            def _():
                fwd(base + others[t], t, 0, d).wait_recv()

    krow = lax.broadcasted_iota(jnp.int32, (chunk, 2 * chunk), 0)
    qcol = lax.rem(lax.broadcasted_iota(jnp.int32, (chunk, 2 * chunk), 1), chunk)

    def attend(items, diagonal=False):
        scores = []
        for tile, blocks in items:
            row = []
            for span, a in blocks:
                raw = nt(kvb[span, a, :chunk], qs[tile])
                row.append(jnp.where(krow <= qcol, raw, -jnp.inf) if diagonal else raw)
            scores.append(row)
        for (tile, blocks), row in zip(items, scores):
            old = peak[tile]
            top = old
            for raw in row:
                top = jnp.maximum(top, jnp.max(raw, axis=0, keepdims=True))
            rescale = jnp.exp(old - top)
            total = None
            weighted = None
            for (span, a), raw in zip(blocks, row):
                e = jnp.exp(raw - top[:1])
                sums = jnp.sum(e.reshape(chunk // 8, 8, 2 * chunk), axis=0)
                turned = jnp.concatenate(
                    [kvb[span, a, chunk + c * val : chunk + (c + 1) * val] for c in range(chunk // 128)],
                    axis=1)
                got = nn(turned, e.astype(BF16))
                total = sums if total is None else total + sums
                weighted = got if weighted is None else weighted + got
            peak[tile] = top
            den[tile] = den[tile] * rescale + total
            acc[tile] = acc[tile] * rescale[:1] + weighted

    def tile_of(t, d):
        return t * nchip + part(d)

    def whole_slots(i):
        slot_t = jnp.where(core == 0, 1, jnp.minimum(i, 1))
        slot = jnp.where(core == 0, i, jnp.maximum(i - 1, 0))
        return slot_t, slot

    def prior_keys(queries_d, keys_d, fresh):
        @pl.loop(0, g)
        def _(back):
            first = SQUARE * (g - 1 - back)
            for group in range(2):
                slots = held if group == 0 else others
                spans = [first + slots[t] for t in range(2)]
                if fresh:
                    for t in range(2):
                        if group == 0:
                            take(spans[t], t, keys_d, False)
                            fwd(spans[t], t, 1 + back, keys_d).start()
                        else:
                            take(spans[t], t, keys_d, False)
                for e in queries_d:
                    attend([(tile_of(t, e), [(span, part(keys_d)) for span in spans]) for t in range(2)])

    def own_whole(queries_d, keys_d):

        @pl.loop(0, SQUARE - 1)
        def _(i):
            slot_t, slot = whole_slots(i)
            attend([(slot_t * nchip + part(e), [(base + slot, part(keys_d))]) for e in queries_d])

    take_own(0)
    attend([(tile_of(t, 0), [(base + held[t], part(0))]) for t in range(2)], diagonal=True)
    take_own_pair(0)
    own_whole([0], 0)

    for d in range(1, nchip):
        other = part(d)
        for half in range(2):
            landed(other * 2 + core, half)
            to_pair(other * 2 + core, half)
        for half in range(2):
            landed(other * 2 + 1 - core, half)
        project(d)
    for d in range(1, nchip):
        project_ret(d)

    blk = BLOCK
    nblk = rows // blk
    rkw = rheads * hd
    tt = lax.broadcasted_iota(jnp.int32, (blk, blk), 0)
    uu = lax.broadcasted_iota(jnp.int32, (blk, blk), 1)
    rlane = lax.broadcasted_iota(jnp.int32, (blk, rkw), 1)
    srow = lax.broadcasted_iota(jnp.int32, (rkw, val), 0)
    decays = []
    span_state = jnp.zeros((rkw, val), F32)
    span_logs = []
    for h in range(rheads):
        ours = (rlane >= h * hd) & (rlane < (h + 1) * hd)
        keep = (srow >= h * hd) & (srow < (h + 1) * hd)
        state = jnp.zeros((rkw, val), F32)
        log_all = jnp.zeros((1, 1), F32)
        for n in range(nblk):
            at = slice(n * blk, (n + 1) * blk)
            row = log_ref[h : h + 1, at]
            full = jnp.broadcast_to(row, (blk, blk))
            c_col = jnp.sum(jnp.where(uu <= tt, full, 0.0), axis=1, keepdims=True)
            l_col = jnp.sum(jnp.where(uu == tt, full, 0.0), axis=1, keepdims=True)
            c_row = jnp.sum(jnp.where(tt <= uu, l_col, 0.0), axis=0, keepdims=True)
            last = c_col[blk - 1 : blk, :]
            query = jnp.where(ours, rbuf[at, :rkw].astype(F32), 0.0)
            keys = rbuf[at, rkw : 2 * rkw]
            values = rbuf[at, 2 * rkw + h * val : 2 * rkw + (h + 1) * val]
            raw = nt(query.astype(BF16), keys)
            gap = jnp.where(uu <= tt, c_col - c_row, -jnp.inf)
            g_mat = (raw * hd ** (-0.5) * jnp.exp(gap)).astype(BF16)
            rmid[h, at, :] = nn(g_mat, values)
            kd = (keys.astype(F32) * hd ** (-0.5) * jnp.exp(last - c_col)).astype(BF16)
            new = jnp.where(keep, tn(kd, values), 0.0)
            upd[h, n] = new
            state = jnp.exp(last) * state + new
            log_all = log_all + last
            decays.append((c_col, last))
        span_state = span_state + state
        span_logs.append(log_all)
    sts[me, :rkw, :] = span_state.astype(BF16)
    for h in range(rheads):
        wide = jnp.broadcast_to(span_logs[h], (16, val))
        hi = wide.astype(BF16)
        sts[me, rkw + 32 * h : rkw + 32 * h + 16, :] = hi
        sts[me, rkw + 32 * h + 16 : rkw + 32 * h + 32, :] = (wide - hi.astype(F32)).astype(BF16)

    @pl.when(first_up)
    def _():
        st_copy(0, me, sem_zs, up).start()

    @pl.when(b == 0)
    def _():
        st_copy(0, me, sem_ys, side).start()

    prior_keys([0], 0, True)
    relay(1)

    for d in range(1, nchip):
        take_own(d)
        if d == 1 and npair > 2:
            relay(2)
        for e in range(d):
            prior_keys([d], e, False)
            own_whole([d], e)
            high = jnp.maximum(part(d), part(e))
            low = jnp.minimum(part(d), part(e))
            attend([(t * nchip + high, [(base + held[t], low)]) for t in range(2)])
        attend([(tile_of(t, d), [(base + held[t], part(d))]) for t in range(2)], diagonal=True)
        take_own_pair(d)
        own_whole(list(range(d + 1)), d)
        if d == 1:

            @pl.loop(3, npair)
            def _(i):
                relay(i)

            first = []
            for h in range(rheads):
                parts = ([jnp.zeros((hd, val), F32)] * h + [init_ref[h]]
                         + [jnp.zeros((hd, val), F32)] * (rheads - 1 - h))
                first.append(jnp.concatenate(parts, axis=0) if rheads > 1 else parts[0])

            @pl.loop(1, npair + 1)
            def _(i):
                jy = 2 * (p - i + 1) + 1 - b

                @pl.when((i - 1 <= p) & ((b == 1) | (i > 1)))
                def _():
                    st_copy(i, jy, sem_ys, side).wait_recv()

            def join(j, states):
                out = []
                for h in range(rheads):
                    keep = (srow >= h * hd) & (srow < (h + 1) * hd)
                    low = rkw + 32 * h
                    log = sts[j, low : low + 16, :].astype(F32) + sts[j, low + 16 : low + 32, :].astype(F32)
                    piece = jnp.where(keep, sts[j, :rkw, :].astype(F32), 0.0)
                    out.append(jnp.exp(log[:1, :]) * states[h] + piece)
                return tuple(out)

            carried = lax.fori_loop(0, me, join, tuple(first))
            for h in range(rheads):
                state = carried[h]
                for n in range(nblk):
                    at = slice(n * blk, (n + 1) * blk)
                    c_col, last = decays[h * nblk + n]
                    query = rbuf[at, :rkw].astype(F32) * jnp.exp(c_col)
                    result = rmid[h, at, :] + nn(query, state, precision=HIGHEST)
                    if n + 1 < nblk:
                        state = jnp.exp(last) * state + upd[h, n]
                    mixr[at, h * val : (h + 1) * val] = head_norm(result).astype(BF16)
        prior_keys(list(range(d + 1)), d, True)

    lam_copy(1 - core).wait_recv()
    lam = lamv[head_core, pl.ds(pl.multiple_of(8 * head_no, 8), 8), :][:1, :1]

    def d_copy(t, d):
        where = {"sp": base + held[t], "tp": chip * 2 + head_core}
        return remote(dsend.at[t, part(d)], dret.at[head_no, part(d)], ds_sem.at[t, d],
                      rd_sem.at[head_no, d], where)

    def d_local(t, d):
        return pltpu.make_async_copy(dsend.at[t, part(d)], dret.at[head_no, part(d)],
                                     rd_sem.at[head_no, d])

    def home(t):
        return (held[t] == s) & (head_core == core)

    targets = list(range(1, nchip)) + [0]
    for d in targets:
        for t in range(2):
            tile = tile_of(t, d)
            scale = 1.0 / jnp.sum(den[tile], axis=0, keepdims=True)
            out = acc[tile] * scale
            merged = out[:, :chunk] - lam * out[:, chunk:]
            square = jnp.mean(merged * merged, axis=0, keepdims=True)
            normed = (merged * lax.rsqrt(square + HEAD_EPS)).T
            dsend[t, part(d)] = (normed * gain_ref[...] * DIFF_SCALE).astype(BF16)

            @pl.when(home(t))
            def _():
                d_local(t, d).start()

            @pl.when(jnp.logical_not(home(t)))
            def _():
                d_copy(t, d).start()

    for load in out_loads:
        load.wait()

    width = out_ref.shape[1]
    cut = mine.shape[2]
    npiece = width // cut

    def returned(d):
        for h in range(heads):
            here = stays(h)

            @pl.when(here)
            def _():
                d_local(0, d).wait()

            @pl.when(jnp.logical_not(here))
            def _():
                remote(dret.at[h, part(d)], dret.at[h, part(d)], ds_sem.at[0, d], rd_sem.at[h, d],
                       pair).wait_recv()

    def partial(which, half, n):
        inner = pl.ds(pl.multiple_of(half * own_rows, own_rows), own_rows)
        owner = which * 2 + half
        rest = mixr[pl.ds(pl.multiple_of(owner * own_rows, own_rows), own_rows), :]
        left = jnp.concatenate([dret[h, which, inner, :] for h in range(heads)] + [rest], axis=1)
        return nn(left, wobuf[:, n * cut : (n + 1) * cut])

    def pair_copy(d, n):
        return remote(mine.at[d * npiece + n], from_pair.at[d * npiece + n], mpair_send.at[d, n],
                      mpair_recv.at[d, n], pair)

    def chip_copy(d, n):
        there = lax.rem(chip + d, nchip) * 2 + core
        return remote(sent.at[d * npiece + n], from_chip.at[d * npiece + n], mchip_send.at[d, n],
                      mchip_recv.at[d, n], {"tp": there})

    for d in targets:
        which = lax.rem(chip + d, nchip)
        returned((nchip - d) % nchip)
        for n in range(npiece):
            mine[d * npiece + n] = partial(which, 1 - core, n).astype(BF16)
            pair_copy(d, n).start()
        if d:
            for n in range(npiece):
                ours = partial(which, core, n)
                pair_copy(d, n).wait_recv()
                sent[d * npiece + n] = (ours + from_pair[d * npiece + n].astype(F32)).astype(BF16)
                chip_copy(d, n).start()
    for n in range(npiece):
        total = partial(chip, core, n)
        pair_copy(0, n).wait_recv()
        total = total + from_pair[n].astype(F32)
        for d in range(1, nchip):
            chip_copy(d, n).wait_recv()
            total = total + from_chip[d * npiece + n].astype(F32)
        out_ref[:, n * cut : (n + 1) * cut] = total.astype(BF16)

    for copy in copies:
        copy.wait_send()

    for d in range(nchip):
        for h in range(heads):

            @pl.when(jnp.logical_not(stays(h)))
            def _():
                q_copy(h, d).wait_send()
                kv_copy(h, d, 0).wait_send()

        for dg in range(1, ngroup):

            @pl.when(g + dg < ngroup)
            def _():
                for h in range(heads):
                    kv_copy(h, d, dg).wait_send()

        for t in range(2):

            @pl.when(needs(t))
            def _():
                fwd(base + held[t], t, 0, d).wait_send()

            @pl.when(jnp.logical_not(home(t)))
            def _():
                d_copy(t, d).wait_send()

        @pl.loop(0, g)
        def _(back):
            for t in range(2):
                fwd(SQUARE * (g - 1 - back) + held[t], t, 1 + back, d).wait_send()

    @pl.loop(0, npair)
    def _(i):
        j = 2 * (p - i) + b

        @pl.when((i <= p) & first_up)
        def _():
            st_copy(i, j, sem_zs, up).wait_send()

        @pl.when((i <= p) & ((i > 0) | (b == 0)))
        def _():
            st_copy(i, j, sem_ys, side).wait_send()

    for d in targets:
        for n in range(npiece):
            pair_copy(d, n).wait_send()
            if d:
                chip_copy(d, n).wait_send()


VMEM = pl.BlockSpec(memory_space=pltpu.VMEM)
ANY = pl.BlockSpec(memory_space=pl.ANY)
SMEM = pl.BlockSpec(memory_space=pltpu.SMEM)
DMA = pltpu.SemaphoreType.DMA


def params(number):
    return pltpu.CompilerParams(
        collective_id=number, has_side_effects=True, vmem_limit_bytes=VMEM_LIMIT
    )


def on_device(nsp, ntp, tokens, norm_gain, w_query_one, w_query_two, w_key_one, w_key_two, w_value,
              mix_lambda, head_gain, w_ret_query, w_ret_key, w_ret_value, retain_log, init_state,
              w_out_diff, w_out_ret):
    weights = (w_query_one, w_query_two, w_key_one, w_key_two, w_value, w_ret_query, w_ret_key, w_ret_value)
    widths = tuple(w.shape[1] for w in weights)
    own_rows, model = tokens.shape
    rows = own_rows * ntp
    nchip = ntp // 2
    npair = nsp // 2
    ngroup = nsp // SQUARE
    chunk = rows // nchip
    heads = mix_lambda.shape[0]
    rheads, hd, val = init_state.shape
    kw = widths[2]
    width = w_out_diff.shape[1]
    npiece = 4
    cut = width // npiece
    return pl.pallas_call(
        functools.partial(layer_kernel, nsp, ntp, widths, heads, rheads),
        out_shape=jax.ShapeDtypeStruct((own_rows, width), BF16),
        in_specs=[SMEM] + [VMEM] * 5 + [ANY] * (len(weights) + 2),
        out_specs=VMEM,
        scratch_shapes=[
            pltpu.VMEM((ntp, own_rows, model), BF16),
            pltpu.VMEM((model, sum(widths)), BF16),
            pltpu.VMEM((w_out_diff.shape[0] + w_out_ret.shape[0], width), BF16),
            pltpu.VMEM((heads, nchip, chunk, kw), BF16),
            pltpu.VMEM((heads, nchip, 2 * chunk, kw), BF16),
            pltpu.VMEM((nsp, nchip, 2 * chunk, kw), BF16),
            pltpu.VMEM((2, nchip, chunk, kw), BF16),
            pltpu.VMEM((2 * nchip, 2 * chunk, kw), BF16),
            pltpu.VMEM((2, 8 * heads, 128), F32),
            pltpu.VMEM((2 * nchip, 8, 2 * chunk), F32),
            pltpu.VMEM((2 * nchip, 8, 2 * chunk), F32),
            pltpu.VMEM((2 * nchip, val, 2 * chunk), F32),
            pltpu.VMEM((2, nchip, chunk, val), BF16),
            pltpu.VMEM((heads, nchip, chunk, val), BF16),
            pltpu.VMEM((nsp, rheads * hd + 32 * rheads, val), BF16),
            pltpu.VMEM((rows, sum(widths[5:])), BF16),
            pltpu.VMEM((rheads, rows, val), F32),
            pltpu.VMEM((rheads, rows // BLOCK, rheads * hd, val), F32),
            pltpu.VMEM((rows, rheads * val), BF16),
            pltpu.VMEM((nchip * npiece, own_rows, cut), BF16),
            pltpu.VMEM((nchip * npiece, own_rows, cut), BF16),
            pltpu.VMEM((nchip * npiece, own_rows, cut), BF16),
            pltpu.VMEM((nchip * npiece, own_rows, cut), BF16),
            DMA((len(weights) + 2,)),
            DMA((2,)),
            DMA((nchip, 2)),
            DMA((nchip, 2)),
            DMA((ntp, 2)),
            DMA((heads, nchip)),
            DMA((heads, nchip)),
            DMA((max(ngroup - 1, 1), heads, nchip)),
            DMA((ngroup, 2, nchip)),
            DMA((2, nchip)),
            DMA((nsp, nchip)),
            DMA((2, nchip)),
            DMA((heads, nchip)),
            DMA((npair + 1,)),
            DMA((npair + 1,)),
            DMA((nsp,)),
            DMA((nchip, npiece)),
            DMA((nchip, npiece)),
            DMA((nchip, npiece)),
            DMA((nchip, npiece)),
        ],
        compiler_params=params(0),
        name="layer",
    )(mix_lambda, tokens, norm_gain[None, :], head_gain[None, :], retain_log, init_state, *weights,
      w_out_diff, w_out_ret)


def solution(mesh):
    in_specs = (
        P(("sp", "tp"), None),
        P(),
        P(None, "tp"),
        P(None, "tp"),
        P(None, "tp"),
        P(None, "tp"),
        P(None, "tp"),
        P("tp"),
        P(),
        P(None, "tp"),
        P(None, "tp"),
        P(None, "tp"),
        P("tp", "sp"),
        P("tp", None, None),
        P("tp", None),
        P("tp", None),
    )
    body = functools.partial(on_device, mesh.shape["sp"], mesh.shape["tp"])
    return jax.shard_map(
        body, mesh=mesh, in_specs=in_specs, out_specs=P(("sp", "tp"), None), check_vma=False
    )
```

time: 85.3 us -> 77 us (0.903)
  the two profiles are of different devices: /device:TPU:29 before, /device:TPU:17 now
where the time goes in v1:
time: 77 us; the launch traced here: 76.3 us
  Pallas kernels  74.4 us (97%)
  local copies, waits for them, and re-layouts  1.88 us (2%)
    pallas_call x1, Pallas kernels, on_device(): pl.pallas_call(functools.partial(layer_kernel, nsp, ntp, widths, heads, r...  74.4 us
    unnamed x1, local copies, waits for them, and re-layouts  1.88 us

profile of v1, /device:TPU:17, one launch (start us, length us, event | category | flops | bytes accessed | tf_op | source)
XLA Modules:
  0.0 76.3 jit_solution(18186351360228882712)
XLA Ops:
  0.0 74.4 %layer.1 = bf16[128,2048]{1,0:T(8,128)(2,1)} custom-call(f32[2]{0:T(128)} %lam_ref.1, bf16[128,2048]{1,0:T(8,128)(2,1)} %tokens_ref.1, f32[1,2048]{1,0:T(1,128)} %bitcast.2, f32[1,128]{1,0:T(1,128)} %bitcast.3, f32[2,512]{1,0:T(2,128)} %log_ref.1, f32[2,64,128]{2,1,0:T(8,128)} %init_ref.1, bf16[2048,128]{1,0:T(8,128)(2,1)} %refs_0_.1, ...), custom_call_target="tpu_custom_call" | custom-call | tf_op jit(solution)/shard_map/layer/pallas_call | solution.py:691
  74.4 1.9 %copy.18 = bf16[128,2048]{1,0:T(8,128)(2,1)} copy(bf16[128,2048]{1,0:T(8,128)(2,1)} %layer.1) | data formatting | bytes 1048576

commit v2 on v1

v2 whole, which is shorter than its diff:
```python
import functools

import jax
import jax.numpy as jnp
from jax import lax
from jax.experimental import pallas as pl
from jax.experimental.pallas import tpu as pltpu
from jax.sharding import PartitionSpec as P

BLOCK = 256
SQUARE = 4
NORM_EPS = 1e-06
HEAD_EPS = 1e-05
DIFF_SCALE = 0.8
HIGHEST = lax.Precision.HIGHEST
MESH = pl.DeviceIdType.MESH
F32 = jnp.float32
BF16 = jnp.bfloat16
VMEM_LIMIT = 60 * 1024 * 1024


def remote(src, dst, send, recv, where):
    return pltpu.make_async_remote_copy(
        src_ref=src, dst_ref=dst, send_sem=send, recv_sem=recv,
        device_id=where, device_id_type=MESH,
    )


def scoped(name):
    def wrap(step):
        def run(*args, **kw):
            with jax.named_scope(name):
                return step(*args, **kw)
        return run
    return wrap


def head_norm(values):
    return values * lax.rsqrt(jnp.mean(values * values, axis=-1, keepdims=True) + HEAD_EPS)


def nn(a, b, **kw):
    return lax.dot_general(a, b, (((1,), (0,)), ((), ())), preferred_element_type=F32, **kw)


def nt(a, b):
    return lax.dot_general(a, b, (((1,), (1,)), ((), ())), preferred_element_type=F32)


def tn(a, b):
    return lax.dot_general(a, b, (((0,), (0,)), ((), ())), preferred_element_type=F32)


def layer_kernel(nsp, ntp, widths, heads, rheads, lam_ref, tokens_ref, ngain_ref, gain_ref, log_ref,
                 init_ref, *refs):
    nw = len(widths)
    w_refs = refs[:nw]
    wd_ref, wr_ref, out_ref = refs[nw : nw + 3]
    (gat, wbuf, wobuf, wx, sndq, sndkv, kvb, qraw, qs, lamv, peak, den, acc, dsend, dret, sts, rbuf,
     decay, along, rmid, upd, mixr, mine, sent, from_pair, from_chip, wsem, lsem, pair_send, cross_send,
     grecv, wx_send, wx_side, wx_recv, sq_sem, skv_sem, inter_sem, fwd_sem, rq_sem, rkv_sem, ds_sem,
     rd_sem, st_send, st_up, st_on, st_recv, mpair_send, mpair_recv, mchip_send, mchip_recv) = refs[nw + 3 :]
    me = lax.axis_index("sp")
    b = lax.rem(me, 2)
    ngroup = nsp // SQUARE
    g = me // SQUARE
    s = lax.rem(me, SQUARE)
    side = {"sp": me + 1 - 2 * b}
    tme = lax.axis_index("tp")
    core = lax.rem(tme, 2)
    chip = tme // 2
    nchip = ntp // 2
    tpair = tme + 1 - 2 * core
    pair = {"tp": tpair}
    own_rows = tokens_ref.shape[0]
    rows = own_rows * ntp
    chunk = rows // nchip
    kw = widths[2]
    hd = kw // heads
    val = gain_ref.shape[1]

    held = (core, SQUARE - 1 - core)
    others = (1 - core, 2 + core)
    land = lax.rem((s + 1) // 2, 2)
    head_core = s // 2
    head_no = lax.rem(s, 2)
    base = SQUARE * g

    barrier = pltpu.get_barrier_semaphore()

    def greet(where):
        pl.semaphore_signal(barrier, inc=1, device_id=where, device_id_type=MESH)

    for k in range(1, ntp):
        greet({"tp": lax.rem(tme + k, ntp)})
    for k in range(1, SQUARE):
        for n in range(ntp):
            greet({"sp": base + lax.rem(s + k, SQUARE), "tp": n})
    for dg in range(1, ngroup):

        @pl.when(g + dg < ngroup)
        def _():
            for h in range(2):
                greet({"sp": base + SQUARE * dg + 2 * core + h, "tp": chip * 2 + land})
            greet({"sp": me + SQUARE * dg})

        @pl.when(g >= dg)
        def _():
            for t in range(2):
                greet({"sp": base - SQUARE * dg + held[t], "tp": chip * 2 + head_core})
            greet({"sp": me - SQUARE * dg})

    order = (0, 1, 2, 3, 4, 5, 6, 7)
    starts = [sum(widths[:n]) for n in range(nw)]
    loads = {}
    for n in order:
        at = starts[n]
        loads[n] = pltpu.make_async_copy(w_refs[n], wbuf.at[:, at : at + widths[n]], wsem.at[n])
        loads[n].start()
    depth = wd_ref.shape[0]
    out_loads = [
        pltpu.make_async_copy(wd_ref, wobuf.at[:depth], wsem.at[nw]),
        pltpu.make_async_copy(wr_ref, wobuf.at[depth:], wsem.at[nw + 1]),
    ]
    for load in out_loads:
        load.start()
    floats = tokens_ref[...].astype(F32)
    gat[tme] = (
        floats * lax.rsqrt(jnp.mean(floats * floats, axis=-1, keepdims=True) + NORM_EPS) * ngain_ref[...]
    ).astype(BF16)
    for h in range(heads):
        lamv[core, 8 * h : 8 * h + 8, :] = jnp.full((8, 128), lam_ref[h], F32)
    pl.semaphore_wait(barrier, (ntp - 1) + (SQUARE - 1) * ntp + 3 * (ngroup - 1))
    copies = []

    def begin(copy):
        copies.append(copy)
        copy.start()

    def slab(which, half):
        return gat.at[which, pl.ds(half * (own_rows // 2), own_rows // 2)]

    def crossing():
        for d in range(1, nchip):
            there = {"tp": lax.rem(chip + d, nchip) * 2 + core}
            for half in range(2):
                yield remote(slab(tme, half), slab(tme, half), cross_send.at[d, half],
                             grecv.at[tme, half], there)

    def cross(which):
        @pl.when(core == which)
        def _():
            for copy in crossing():
                copy.start()

    cross(0)
    copies.extend(crossing())

    def pair_slab(which, half):
        return remote(slab(which, half), slab(which, half), pair_send.at[which // 2, half],
                      grecv.at[which, half], pair)

    @scoped("landed")
    def landed(which, half):
        remote(slab(which, half), slab(which, half), pair_send.at[which // 2, half],
               grecv.at[which, half], pair).wait_recv()

    def lam_copy(who):
        return remote(lamv.at[who], lamv.at[who], lsem.at[0], lsem.at[1], pair)

    def part(d):
        return lax.rem(chip + nchip - d, nchip)

    def keys_at(d):
        return pl.ds(pl.multiple_of(part(d) * chunk, chunk), chunk)

    def steps(d):
        return ((0, 0, 2),) if d == 0 else ((2 * d - 1, 0, 1), (2 * d, 1, 1))

    def q_rows(ref, at, step):
        return ref.at[at, pl.ds(step[1] * own_rows, step[2] * own_rows)]

    def kv_rows(ref, at, step):
        return ref.at[at, pl.ds(step[1] * 2 * own_rows, step[2] * 2 * own_rows)]

    def q_copy(h, d, step):
        where = {"sp": base + 2 * core + h, "tp": chip * 2 + land}
        return remote(q_rows(sndq.at[h], part(d), step), q_rows(qraw.at[s // 2], part(d), step),
                      sq_sem.at[h, step[0]], rq_sem.at[s // 2, d], where)

    def kv_copy(h, d, dg, step):
        where = {"sp": base + SQUARE * dg + 2 * core + h, "tp": chip * 2 + land}
        sem = skv_sem.at[h, step[0]] if dg == 0 else inter_sem.at[dg - 1, h, step[0]]
        return remote(kv_rows(sndkv.at[h], part(d), step), kv_rows(kvb.at[me], part(d), step), sem,
                      rkv_sem.at[me, d], where)

    def q_local(h, d, step):
        return pltpu.make_async_copy(q_rows(sndq.at[h], part(d), step),
                                     q_rows(qraw.at[s // 2], part(d), step), rq_sem.at[s // 2, d])

    def kv_local(h, d, step):
        return pltpu.make_async_copy(kv_rows(sndkv.at[h], part(d), step),
                                     kv_rows(kvb.at[me], part(d), step), rkv_sem.at[me, d])

    def stays(h):
        return (2 * core + h == s) & (land == core)

    def fwd(span, t, dg, d):
        piece = kvb.at[span, part(d)]
        return remote(piece, piece, fwd_sem.at[dg, t, d], rkv_sem.at[span, d], pair)

    lane = lax.broadcasted_iota(jnp.int32, (chunk, 128), 1)

    @scoped("project")
    def project(d, step):
        number, first, slabs = step
        count = slabs * own_rows
        rows_in = gat[pl.ds(part(d) * 2 + first, slabs)].reshape(count, gat.shape[2])
        low = lane[:count] < hd

        def product(lo, hi):
            if d == 0:
                for n in range(lo, hi):
                    loads[n].wait()
            span = sum(widths[lo:hi])
            return nn(rows_in, wbuf[:, starts[lo] : starts[lo] + span]).astype(BF16).astype(F32)

        def by_head(pairs):
            one, two = pairs[:, :kw], pairs[:, kw:]
            return (jnp.where(low, one, pltpu.roll(two, hd, 1)),
                    jnp.where(low, pltpu.roll(one, kw - hd, 1), two))

        queries = by_head(product(0, 2) * hd ** (-0.5))
        for h in range(heads):
            sndq[h, part(d), first * own_rows : first * own_rows + count] = queries[h].astype(BF16)
        keys = by_head(product(2, 4))
        values = product(4, 5)
        for h in range(heads):
            turned = values[:, h * val : (h + 1) * val].T.astype(BF16)
            for c in range(slabs):
                at = 2 * own_rows * (first + c)
                rows_of = slice(c * own_rows, (c + 1) * own_rows)
                sndkv[h, part(d), at : at + own_rows] = keys[h][rows_of].astype(BF16)
                sndkv[h, part(d), at + own_rows : at + 2 * own_rows] = turned[:, rows_of]
        for h in range(heads):

            @pl.when(stays(h))
            def _():
                q_local(h, d, step).start()
                kv_local(h, d, step).start()

            @pl.when(jnp.logical_not(stays(h)))
            def _():
                q_copy(h, d, step).start()
                kv_copy(h, d, 0, step).start()

    def to_later(d, step, only=None):
        for dg in range(1, ngroup):
            goes = g + dg < ngroup
            if only is not None:
                goes = goes & (core == only)

            @pl.when(goes)
            def _():
                for h in range(heads):
                    kv_copy(h, d, dg, step).start()

    @scoped("project_ret")
    def project_ret(d):
        both = gat[pl.ds(part(d) * 2, 2)].reshape(chunk, gat.shape[2])
        if d == 0:
            for n in range(5, 8):
                loads[n].wait()
        span = sum(widths[5:8])
        for c in range(0, span, 256):
            rbuf[keys_at(d), c : c + 256] = nn(
                both, wbuf[:, starts[5] + c : starts[5] + c + 256]).astype(BF16)

    wpiece = depth // 4

    def w_rows(ref, half, n):
        return ref.at[pl.ds(pl.multiple_of(half * 2 * wpiece, 2 * wpiece) + n * wpiece, wpiece)]

    def w_cross(d, n):
        there = {"tp": lax.rem(chip + d, nchip) * 2 + core}
        return remote(w_rows(wobuf, b, n), w_rows(wx.at[nchip - d - 1], b, n), wx_send.at[d - 1, n],
                      wx_recv.at[nchip - d - 1, b, n], there)

    def w_side(d, half, n):
        piece = w_rows(wx.at[d - 1], half, n)
        return remote(piece, piece, wx_side.at[d - 1, n], wx_recv.at[d - 1, half, n], side)

    @scoped("w_pass")
    def w_pass(n):
        for d in range(1, nchip):
            w_side(d, b, n).wait_recv()
            w_side(d, b, n).start()

    for half in range(2):
        begin(pair_slab(tme, half))
    for d in range(1, nchip):
        for half in range(2):
            copies.append(pair_slab(part(d) * 2 + core, half))
    begin(lam_copy(core))
    peak[...] = jnp.full(peak.shape, -jnp.inf, F32)
    den[...] = jnp.zeros(den.shape, F32)
    acc[...] = jnp.zeros(acc.shape, F32)
    for half in range(2):
        landed(tpair, half)
    project(0, steps(0)[0])
    to_later(0, steps(0)[0])
    cross(1)
    project_ret(0)

    blk = BLOCK
    nblk = rows // blk
    rkw = rheads * hd
    tt = lax.broadcasted_iota(jnp.int32, (blk, blk), 0)
    uu = lax.broadcasted_iota(jnp.int32, (blk, blk), 1)
    rlane = lax.broadcasted_iota(jnp.int32, (blk, rkw), 1)
    srow = lax.broadcasted_iota(jnp.int32, (rkw, val), 0)

    def ours(iota, h):
        return (iota >= h * hd) & (iota < (h + 1) * hd)

    @scoped("decays")
    def decays():
        for h in range(rheads):
            for n in range(nblk):
                row = log_ref[h : h + 1, n * blk : (n + 1) * blk]
                full = jnp.broadcast_to(row, (blk, blk))
                c_col = jnp.sum(jnp.where(uu <= tt, full, 0.0), axis=1, keepdims=True)
                l_col = jnp.sum(jnp.where(uu == tt, full, 0.0), axis=1, keepdims=True)
                c_row = jnp.sum(jnp.where(tt <= uu, l_col, 0.0), axis=0, keepdims=True)
                decay[h, n] = jnp.exp(jnp.where(uu <= tt, c_col - c_row, -jnp.inf))
                along[h, n] = jnp.broadcast_to(c_col, (blk, 128))

    def blocks_of(d):
        for i in range(chunk // blk):
            n = part(d) * (chunk // blk) + i
            yield n, pl.ds(pl.multiple_of(n * blk, blk), blk)

    @scoped("ret_states")
    def ret_states(d):
        for n, at in blocks_of(d):
            keys = rbuf[at, rkw : 2 * rkw].astype(F32) * hd ** (-0.5)
            for h in range(rheads):
                c = along[h, n]
                kd = (keys * jnp.exp(c[blk - 1 : blk, :1] - c[:, :1])).astype(BF16)
                values = rbuf[at, 2 * rkw + h * val : 2 * rkw + (h + 1) * val]
                upd[h, n] = jnp.where(ours(srow, h), tn(kd, values), 0.0)

    @scoped("ret_inner")
    def ret_inner(d):
        for n, at in blocks_of(d):
            keys = rbuf[at, rkw : 2 * rkw]
            for h in range(rheads):
                query = jnp.where(ours(rlane, h), rbuf[at, :rkw].astype(F32), 0.0)
                raw = nt(query.astype(BF16), keys)
                weights = (raw * hd ** (-0.5) * decay[h, n]).astype(BF16)
                rmid[h, at, :] = nn(weights, rbuf[at, 2 * rkw + h * val : 2 * rkw + (h + 1) * val])

    logrow = lax.broadcasted_iota(jnp.int32, (16, val), 0)

    def put_state(slot, state, logs):
        sts[slot, :rkw, :] = state.astype(BF16)
        tile = jnp.zeros((16, val), F32)
        for h in range(rheads):
            wide = jnp.broadcast_to(logs[h], (16, val))
            hi = wide.astype(BF16).astype(F32)
            tile = jnp.where(logrow == 2 * h, hi, tile)
            tile = jnp.where(logrow == 2 * h + 1, wide - hi, tile)
        sts[slot, rkw:, :] = tile.astype(BF16)

    def join(slot, states):
        piece = sts[slot, :rkw, :].astype(F32)
        logs = sts[slot, rkw:, :].astype(F32)
        return tuple(
            jnp.exp(logs[2 * h : 2 * h + 1] + logs[2 * h + 1 : 2 * h + 2]) * states[h]
            + jnp.where(ours(srow, h), piece, 0.0)
            for h in range(rheads)
        )

    def st_copy(k):
        return remote(sts.at[me], sts.at[me], st_send.at[k], st_recv.at[me],
                      {"sp": base + lax.rem(s + k, SQUARE)})

    def st_later(dg):
        return remote(sts.at[me], sts.at[me], st_up.at[dg], st_recv.at[me], {"sp": me + SQUARE * dg})

    def st_pass(back, k):
        span = me - SQUARE * (back + 1)
        return remote(sts.at[span], sts.at[span], st_on.at[back, k], st_recv.at[span],
                      {"sp": base + lax.rem(s + k, SQUARE)})

    def st_wait(span):
        remote(sts.at[span], sts.at[span], st_send.at[0], st_recv.at[span], pair).wait_recv()

    @scoped("span_state")
    def span_state():
        total = jnp.zeros((rkw, val), F32)
        logs = []
        for h in range(rheads):
            state = jnp.zeros((rkw, val), F32)
            log_all = jnp.zeros((1, 1), F32)
            for n in range(nblk):
                last = along[h, n, blk - 1 : blk, :1]
                state = jnp.exp(last) * state + upd[h, n]
                log_all = log_all + last
            total = total + state
            logs.append(log_all)
        put_state(me, total, logs)
        for k in range(1, SQUARE):

            @pl.when(s + k < SQUARE)
            def _():
                st_copy(k).start()

        for dg in range(1, ngroup):

            @pl.when(g + dg < ngroup)
            def _():
                st_later(dg).start()

    @scoped("pass_states")
    def pass_states():
        @pl.loop(0, g)
        def _(back):
            st_wait(me - SQUARE * (back + 1))
            for k in range(1, SQUARE):
                st_pass(back, k).start()

    @scoped("ret_finish")
    def ret_finish():
        first = []
        for h in range(rheads):
            parts = ([jnp.zeros((hd, val), F32)] * h + [init_ref[h]]
                     + [jnp.zeros((hd, val), F32)] * (rheads - 1 - h))
            first.append(jnp.concatenate(parts, axis=0) if rheads > 1 else parts[0])

        @pl.loop(0, g)
        def _(back):
            for k in range(1, SQUARE):
                st_wait(base - SQUARE * (back + 1) + lax.rem(s + k, SQUARE))

        @pl.loop(0, s)
        def _(slot):
            st_wait(base + slot)

        carried = lax.fori_loop(0, me, join, tuple(first))
        for h in range(rheads):
            state = carried[h]
            for n in range(nblk):
                at = slice(n * blk, (n + 1) * blk)
                c = along[h, n]
                query = rbuf[at, :rkw].astype(F32) * jnp.exp(c[:, :1])
                result = rmid[h, at, :] + nn(query, state, precision=HIGHEST)
                if n + 1 < nblk:
                    state = jnp.exp(c[blk - 1 : blk, :1]) * state + upd[h, n]
                mixr[at, h * val : (h + 1) * val] = head_norm(result).astype(BF16)

    decays()
    ret_states(0)
    ret_inner(0)

    @scoped("take")
    def take(span, t, d, local):
        if local:
            here = (held[t] == s) & (head_core == core)

            @pl.when(here)
            def _():
                pltpu.make_async_copy(sndq.at[0, part(d)], qraw.at[t, part(d)], rq_sem.at[t, d]).wait()
                pltpu.make_async_copy(sndkv.at[0, part(d)], kvb.at[span, part(d)],
                                      rkv_sem.at[span, d]).wait()

            @pl.when(jnp.logical_not(here))
            def _():
                remote(qraw.at[t, part(d)], qraw.at[t, part(d)], sq_sem.at[0, d],
                       rq_sem.at[t, d], pair).wait_recv()
                remote(kvb.at[span, part(d)], kvb.at[span, part(d)], skv_sem.at[0, d],
                       rkv_sem.at[span, d], pair).wait_recv()
        else:
            remote(kvb.at[span, part(d)], kvb.at[span, part(d)], skv_sem.at[0, d],
                   rkv_sem.at[span, d], pair).wait_recv()

    def ready(t, d):
        tile = t * nchip + part(d)
        value = qraw[t, part(d)].astype(F32)
        qs[tile, :chunk] = jnp.where(lane < hd, value, 0.0).astype(BF16)
        qs[tile, chunk:] = jnp.where(lane < hd, 0.0, value).astype(BF16)

    def needs(t):
        return (core == 1) | (t == 0)

    def take_own(d):
        for t in range(2):
            take(base + held[t], t, d, True)

            @pl.when(needs(t))
            def _():
                fwd(base + held[t], t, 0, d).start()

        for t in range(2):
            ready(t, d)

    @scoped("take_own_pair")
    def take_own_pair(d):
        for t in range(2):

            @pl.when((core == 0) | (t == 0))
            def _():
                fwd(base + others[t], t, 0, d).wait_recv()

    krow = lax.broadcasted_iota(jnp.int32, (chunk, 2 * chunk), 0)
    qcol = lax.rem(lax.broadcasted_iota(jnp.int32, (chunk, 2 * chunk), 1), chunk)

    @scoped("attend")
    def attend(items, diagonal=False):
        scores = []
        for tile, blocks in items:
            row = []
            for span, a in blocks:
                keys = jnp.concatenate(
                    [kvb[span, a, 2 * c * own_rows : (2 * c + 1) * own_rows] for c in range(2)], axis=0)
                raw = nt(keys, qs[tile])
                row.append(jnp.where(krow <= qcol, raw, -jnp.inf) if diagonal else raw)
            scores.append(row)
        for (tile, blocks), row in zip(items, scores):
            old = peak[tile]
            top = old
            for raw in row:
                top = jnp.maximum(top, jnp.max(raw, axis=0, keepdims=True))
            rescale = jnp.exp(old - top)
            total = None
            weighted = None
            for (span, a), raw in zip(blocks, row):
                e = jnp.exp(raw - top[:1])
                sums = jnp.sum(e.reshape(chunk // 8, 8, 2 * chunk), axis=0)
                turned = jnp.concatenate(
                    [kvb[span, a, (2 * c + 1) * own_rows : (2 * c + 2) * own_rows] for c in range(2)],
                    axis=1)
                got = nn(turned, e.astype(BF16))
                total = sums if total is None else total + sums
                weighted = got if weighted is None else weighted + got
            peak[tile] = top
            den[tile] = den[tile] * rescale + total
            acc[tile] = acc[tile] * rescale[:1] + weighted

    def tile_of(t, d):
        return t * nchip + part(d)

    def prior_keys(queries_d, keys_d, fresh):
        @pl.loop(0, g)
        def _(back):
            first = SQUARE * (g - 1 - back)
            for group in range(2):
                slots = held if group == 0 else others
                spans = [first + slots[t] for t in range(2)]
                if fresh:
                    for t in range(2):
                        if group == 0:
                            take(spans[t], t, keys_d, False)
                            fwd(spans[t], t, 1 + back, keys_d).start()
                        else:
                            take(spans[t], t, keys_d, False)
                for e in queries_d:
                    attend([(tile_of(t, e), [(span, part(keys_d)) for span in spans]) for t in range(2)])

    def own_whole(queries_d, keys_d):
        third_t, third_slot = 1 - core, 2 * (1 - core)
        at = part(keys_d)
        attend([item for e in queries_d for item in (
            (nchip + part(e), ((base, at), (base + 1, at))),
            (third_t * nchip + part(e), ((base + third_slot, at),)),
        )])

    width = out_ref.shape[1]
    cut = mine.shape[2]
    npiece = width // cut

    def mixed_rows(which, half):
        owner = which * 2 + half
        return mixr[pl.ds(pl.multiple_of(owner * own_rows, own_rows), own_rows), :]

    def pair_copy(d, n):
        return remote(mine.at[d * npiece + n], from_pair.at[d * npiece + n], mpair_send.at[d, n],
                      mpair_recv.at[d, n], pair)

    def chip_copy(d, n):
        there = lax.rem(chip + d, nchip) * 2 + core
        return remote(sent.at[d * npiece + n], from_chip.at[d * npiece + n], mchip_send.at[d, n],
                      mchip_recv.at[d, n], {"tp": there})

    @scoped("ret_reduce")
    def ret_reduce():
        out_loads[1].wait()
        for d in range(1, nchip):
            which = lax.rem(chip + d, nchip)
            for n in range(npiece):
                cols = wobuf[depth:, n * cut : (n + 1) * cut]
                mine[d * npiece + n] = nn(mixed_rows(which, 1 - core), cols).astype(BF16)
                pair_copy(d, n).start()

    @scoped("ret_send")
    def ret_send():
        for d in range(1, nchip):
            which = lax.rem(chip + d, nchip)
            for n in range(npiece):
                cols = wobuf[depth:, n * cut : (n + 1) * cut]
                part_sum = nn(mixed_rows(which, core), cols)
                pair_copy(d, n).wait_recv()
                sent[d * npiece + n] = (part_sum + from_pair[d * npiece + n].astype(F32)).astype(BF16)
                chip_copy(d, n).start()

    def slab_in(d, which):
        index = part(d) * 2 + which
        for half in range(2):
            landed(index, half)

            @pl.when(core == which)
            def _():
                pair_slab(index, half).start()

    for d in range(1, nchip):
        slab_in(d, 0)
        project(d, steps(d)[0])
        to_later(d, steps(d)[0], 0)

    take_own(0)
    attend([(tile_of(t, 0), [(base + held[t], part(0))]) for t in range(2)], diagonal=True)
    take_own_pair(0)
    own_whole([0], 0)

    for d in range(1, nchip):
        slab_in(d, 1)
        if d == nchip - 1:
            out_loads[0].wait()
            for e in range(1, nchip):
                for n in range(2):
                    w_cross(e, n).start()
        project_ret(d)
        ret_states(d)
        if d == nchip - 1:
            span_state()
        project(d, steps(d)[1])
        to_later(d, steps(d)[1], 0)
        if d < nchip - 1:
            for step in steps(d):
                to_later(d, step, 1)
        ret_inner(d)
    prior_keys([0], 0, True)
    pass_states()

    for d in range(1, nchip):
        take_own(d)
        if d == nchip - 1:
            w_pass(0)
            ret_finish()
            ret_reduce()
            w_pass(1)
            ret_send()
            for step in steps(d):
                to_later(d, step, 1)
        for e in range(d):
            prior_keys([d], e, False)
            own_whole([d], e)
            high = jnp.maximum(part(d), part(e))
            low = jnp.minimum(part(d), part(e))
            attend([(t * nchip + high, [(base + held[t], low)]) for t in range(2)])
        attend([(tile_of(t, d), [(base + held[t], part(d))]) for t in range(2)], diagonal=True)
        take_own_pair(d)
        own_whole(list(range(d + 1)), d)
        prior_keys(list(range(d + 1)), d, True)

    lam_copy(1 - core).wait_recv()
    lam = lamv[head_core, pl.ds(pl.multiple_of(8 * head_no, 8), 8), :][:1, :1]

    def d_copy(t, d):
        where = {"sp": base + held[t], "tp": part(d) * 2 + head_core}
        return remote(dsend.at[t, part(d)], dret.at[chip, head_no], ds_sem.at[t, d],
                      rd_sem.at[chip, head_no], where)

    def d_local(t, d):
        return pltpu.make_async_copy(dsend.at[t, part(d)], dret.at[chip, head_no],
                                     rd_sem.at[chip, head_no])

    def home(t, d):
        return (held[t] == s) & (head_core == core) if d == 0 else False

    @scoped("finish")
    def finish(t, d):
        tile = tile_of(t, d)
        scale = 1.0 / jnp.sum(den[tile], axis=0, keepdims=True)
        out = acc[tile] * scale
        merged = out[:, :chunk] - lam * out[:, chunk:]
        square = jnp.mean(merged * merged, axis=0, keepdims=True)
        normed = (merged * lax.rsqrt(square + HEAD_EPS)).T
        dsend[t, part(d)] = (normed * gain_ref[...] * DIFF_SCALE).astype(BF16)
        if d:
            d_copy(t, d).start()
        else:

            @pl.when(home(t, d))
            def _():
                d_local(t, d).start()

            @pl.when(jnp.logical_not(home(t, d)))
            def _():
                d_copy(t, d).start()

    for d in list(range(1, nchip)) + [0]:
        for t in range(2):
            finish(t, d)

    for d in range(1, nchip):
        for n in range(2):
            with jax.named_scope("w_last"):
                w_side(d, 1 - b, n).wait_recv()
    for h in range(heads):
        for d in range(nchip):
            source = lax.rem(chip + d, nchip)
            piece = dret.at[source, h]
            arrival = remote(piece, piece, ds_sem.at[0, d], rd_sem.at[source, h], pair)
            if d:
                with jax.named_scope("d_wait"):
                    arrival.wait_recv()
            else:

                @pl.when(stays(h))
                def _():
                    pltpu.make_async_copy(dsend.at[0, chip], piece, rd_sem.at[source, h]).wait()

                @pl.when(jnp.logical_not(stays(h)))
                def _():
                    with jax.named_scope("d_wait"):
                        arrival.wait_recv()

    def partial(half, n):
        inner = pl.ds(pl.multiple_of(half * own_rows, own_rows), own_rows)
        total = nn(
            jnp.concatenate([dret[chip, h, inner, :] for h in range(heads)] + [mixed_rows(chip, half)], axis=1),
            wobuf[:, n * cut : (n + 1) * cut])
        for d in range(1, nchip):
            source = lax.rem(chip + d, nchip)
            total = total + nn(
                jnp.concatenate([dret[source, h, inner, :] for h in range(heads)], axis=1),
                wx[d - 1, :, n * cut : (n + 1) * cut])
        return total

    for n in range(npiece):
        mine[n] = partial(1 - core, n).astype(BF16)
        pair_copy(0, n).start()
    for n in range(npiece):
        total = partial(core, n)
        with jax.named_scope("p_wait"):
            pair_copy(0, n).wait_recv()
        total = total + from_pair[n].astype(F32)
        for d in range(1, nchip):
            with jax.named_scope("c_wait"):
                chip_copy(d, n).wait_recv()
            total = total + from_chip[d * npiece + n].astype(F32)
        out_ref[:, n * cut : (n + 1) * cut] = total.astype(BF16)

    with jax.named_scope("s_wait"):
        for copy in copies:
            copy.wait_send()

    for d in range(nchip):
        for h in range(heads):

            @pl.when(jnp.logical_not(stays(h)))
            def _():
                for step in steps(d):
                    q_copy(h, d, step).wait_send()
                    kv_copy(h, d, 0, step).wait_send()

        for dg in range(1, ngroup):

            @pl.when(g + dg < ngroup)
            def _():
                for h in range(heads):
                    for step in steps(d):
                        kv_copy(h, d, dg, step).wait_send()

        for t in range(2):

            @pl.when(needs(t))
            def _():
                fwd(base + held[t], t, 0, d).wait_send()

            if d:
                d_copy(t, d).wait_send()
            else:

                @pl.when(jnp.logical_not(home(t, d)))
                def _():
                    d_copy(t, d).wait_send()

        @pl.loop(0, g)
        def _(back):
            for t in range(2):
                fwd(SQUARE * (g - 1 - back) + held[t], t, 1 + back, d).wait_send()

    for d in range(1, nchip):
        for n in range(2):
            w_cross(d, n).wait_send()
            w_side(d, b, n).wait_send()
    for k in range(1, SQUARE):

        @pl.when(s + k < SQUARE)
        def _():
            st_copy(k).wait_send()

        @pl.loop(0, g)
        def _(back):
            st_pass(back, k).wait_send()

    for dg in range(1, ngroup):

        @pl.when(g + dg < ngroup)
        def _():
            st_later(dg).wait_send()

    for d in range(nchip):
        for n in range(npiece):
            pair_copy(d, n).wait_send()
            if d:
                chip_copy(d, n).wait_send()


VMEM = pl.BlockSpec(memory_space=pltpu.VMEM)
ANY = pl.BlockSpec(memory_space=pl.ANY)
SMEM = pl.BlockSpec(memory_space=pltpu.SMEM)
DMA = pltpu.SemaphoreType.DMA


def params(number):
    return pltpu.CompilerParams(
        collective_id=number, has_side_effects=True, vmem_limit_bytes=VMEM_LIMIT
    )


def on_device(nsp, ntp, tokens, norm_gain, w_query_one, w_query_two, w_key_one, w_key_two, w_value,
              mix_lambda, head_gain, w_ret_query, w_ret_key, w_ret_value, retain_log, init_state,
              w_out_diff, w_out_ret):
    weights = (w_query_one, w_query_two, w_key_one, w_key_two, w_value, w_ret_query, w_ret_key, w_ret_value)
    widths = tuple(w.shape[1] for w in weights)
    own_rows, model = tokens.shape
    rows = own_rows * ntp
    nchip = ntp // 2
    ngroup = nsp // SQUARE
    chunk = rows // nchip
    heads = mix_lambda.shape[0]
    rheads, hd, val = init_state.shape
    kw = widths[2]
    width = w_out_diff.shape[1]
    npiece = 4
    cut = width // npiece
    return pl.pallas_call(
        functools.partial(layer_kernel, nsp, ntp, widths, heads, rheads),
        out_shape=jax.ShapeDtypeStruct((own_rows, width), BF16),
        in_specs=[SMEM] + [VMEM] * 5 + [ANY] * (len(weights) + 2),
        out_specs=VMEM,
        scratch_shapes=[
            pltpu.VMEM((ntp, own_rows, model), BF16),
            pltpu.VMEM((model, sum(widths)), BF16),
            pltpu.VMEM((w_out_diff.shape[0] + w_out_ret.shape[0], width), BF16),
            pltpu.VMEM((nchip - 1, w_out_diff.shape[0], width), BF16),
            pltpu.VMEM((heads, nchip, chunk, kw), BF16),
            pltpu.VMEM((heads, nchip, 2 * chunk, kw), BF16),
            pltpu.VMEM((nsp, nchip, 2 * chunk, kw), BF16),
            pltpu.VMEM((2, nchip, chunk, kw), BF16),
            pltpu.VMEM((2 * nchip, 2 * chunk, kw), BF16),
            pltpu.VMEM((2, 8 * heads, 128), F32),
            pltpu.VMEM((2 * nchip, 8, 2 * chunk), F32),
            pltpu.VMEM((2 * nchip, 8, 2 * chunk), F32),
            pltpu.VMEM((2 * nchip, val, 2 * chunk), F32),
            pltpu.VMEM((2, nchip, chunk, val), BF16),
            pltpu.VMEM((nchip, heads, chunk, val), BF16),
            pltpu.VMEM((nsp, rheads * hd + 16, val), BF16),
            pltpu.VMEM((rows, sum(widths[5:])), BF16),
            pltpu.VMEM((rheads, rows // BLOCK, BLOCK, BLOCK), F32),
            pltpu.VMEM((rheads, rows // BLOCK, BLOCK, 128), F32),
            pltpu.VMEM((rheads, rows, val), F32),
            pltpu.VMEM((rheads, rows // BLOCK, rheads * hd, val), F32),
            pltpu.VMEM((rows, rheads * val), BF16),
            pltpu.VMEM((nchip * npiece, own_rows, cut), BF16),
            pltpu.VMEM((nchip * npiece, own_rows, cut), BF16),
            pltpu.VMEM((nchip * npiece, own_rows, cut), BF16),
            pltpu.VMEM((nchip * npiece, own_rows, cut), BF16),
            DMA((len(weights) + 2,)),
            DMA((2,)),
            DMA((nchip, 2)),
            DMA((nchip, 2)),
            DMA((ntp, 2)),
            DMA((nchip - 1, 2)),
            DMA((nchip - 1, 2)),
            DMA((nchip - 1, 2, 2)),
            DMA((heads, 2 * nchip - 1)),
            DMA((heads, 2 * nchip - 1)),
            DMA((max(ngroup - 1, 1), heads, 2 * nchip - 1)),
            DMA((ngroup, 2, nchip)),
            DMA((2, nchip)),
            DMA((nsp, nchip)),
            DMA((2, nchip)),
            DMA((nchip, heads)),
            DMA((SQUARE,)),
            DMA((ngroup,)),
            DMA((ngroup, SQUARE)),
            DMA((nsp,)),
            DMA((nchip, npiece)),
            DMA((nchip, npiece)),
            DMA((nchip, npiece)),
            DMA((nchip, npiece)),
        ],
        compiler_params=params(0),
        name="layer",
    )(mix_lambda, tokens, norm_gain[None, :], head_gain[None, :], retain_log, init_state, *weights,
      w_out_diff, w_out_ret)


def solution(mesh):
    in_specs = (
        P(("sp", "tp"), None),
        P(),
        P(None, "tp"),
        P(None, "tp"),
        P(None, "tp"),
        P(None, "tp"),
        P(None, "tp"),
        P("tp"),
        P(),
        P(None, "tp"),
        P(None, "tp"),
        P(None, "tp"),
        P("tp", "sp"),
        P("tp", None, None),
        P("tp", None),
        P("tp", None),
    )
    body = functools.partial(on_device, mesh.shape["sp"], mesh.shape["tp"])
    return jax.shard_map(
        body, mesh=mesh, in_specs=in_specs, out_specs=P(("sp", "tp"), None), check_vma=False
    )
```

time: 77 us -> 57 us (0.74)
  Pallas kernels: 74.4 us -> 55 us
    pallas_call x1, Pallas kernels: 74.4 us -> 55 us  [on_device(): pl.pallas_call(functools.partial(layer_kernel, nsp, ntp, widths, heads, r...]
where the time goes in v2:
time: 57 us; the launch traced here: 56.9 us
  Pallas kernels  55 us (96%)
  local copies, waits for them, and re-layouts  1.88 us (3%)
    pallas_call x1, Pallas kernels, on_device(): pl.pallas_call(functools.partial(layer_kernel, nsp, ntp, widths, heads, r...  55 us
    unnamed x1, local copies, waits for them, and re-layouts  1.88 us

profile of v2, /device:TPU:17, one launch (start us, length us, event | category | flops | bytes accessed | tf_op | source)
XLA Modules:
  0.0 56.9 jit_solution(6937813086893652276)
XLA Ops:
  0.0 55.0 %layer.1 = bf16[128,2048]{1,0:T(8,128)(2,1)} custom-call(f32[2]{0:T(128)} %lam_ref.1, bf16[128,2048]{1,0:T(8,128)(2,1)} %tokens_ref.1, f32[1,2048]{1,0:T(1,128)} %bitcast.2, f32[1,128]{1,0:T(1,128)} %bitcast.3, f32[2,512]{1,0:T(2,128)} %log_ref.1, f32[2,64,128]{2,1,0:T(8,128)} %init_ref.1, bf16[2048,128]{1,0:T(8,128)(2,1)} %refs_0_.1, ...), custom_call_target="tpu_custom_call" | custom-call | tf_op jit(solution)/shard_map/layer/pallas_call | solution.py:860
  55.0 1.9 %copy.18 = bf16[128,2048]{1,0:T(8,128)(2,1)} copy(bf16[128,2048]{1,0:T(8,128)(2,1)} %layer.1) | data formatting | bytes 1048576

commit v3 on v2

--- a/solution.py
+++ b/solution.py
@@ -57,9 +57,9 @@
     w_refs = refs[:nw]
     wd_ref, wr_ref, out_ref = refs[nw : nw + 3]
     (gat, wbuf, wobuf, wx, sndq, sndkv, kvb, qraw, qs, lamv, peak, den, acc, dsend, dret, sts, rbuf,
-     decay, along, rmid, upd, mixr, mine, sent, from_pair, from_chip, wsem, lsem, pair_send, cross_send,
+     decay, along, rmid, upd, mixr, mine, sent, from_pair, from_chip, kept, outv, wsem, lsem, pair_send, cross_send,
      grecv, wx_send, wx_side, wx_recv, sq_sem, skv_sem, inter_sem, fwd_sem, rq_sem, rkv_sem, ds_sem,
-     rd_sem, st_send, st_up, st_on, st_recv, mpair_send, mpair_recv, mchip_send, mchip_recv) = refs[nw + 3 :]
+     rd_sem, st_send, st_up, st_on, st_recv, mpair_send, mpair_recv, mchip_send, mchip_recv, osem) = refs[nw + 3 :]
     me = lax.axis_index("sp")
     b = lax.rem(me, 2)
     ngroup = nsp // SQUARE
@@ -308,7 +308,7 @@
     for half in range(2):
         landed(tpair, half)
     project(0, steps(0)[0])
-    to_later(0, steps(0)[0])
+    to_later(0, steps(0)[0], 1)
     cross(1)
     project_ret(0)
 
@@ -462,6 +462,7 @@
     decays()
     ret_states(0)
     ret_inner(0)
+    to_later(0, steps(0)[0], 0)
 
     @scoped("take")
     def take(span, t, d, local):
@@ -579,9 +580,14 @@
     cut = mine.shape[2]
     npiece = width // cut
 
-    def mixed_rows(which, half):
-        owner = which * 2 + half
-        return mixr[pl.ds(pl.multiple_of(owner * own_rows, own_rows), own_rows), :]
+    def mixed_rows(which):
+        return mixr[pl.ds(pl.multiple_of(which * chunk, chunk), chunk), :]
+
+    def split(d, n, full):
+        first, second = full[:own_rows], full[own_rows:]
+        mine[d * npiece + n] = jnp.where(core == 0, second, first).astype(BF16)
+        kept[d * npiece + n] = jnp.where(core == 0, first, second)
+        pair_copy(d, n).start()
 
     def pair_copy(d, n):
         return remote(mine.at[d * npiece + n], from_pair.at[d * npiece + n], mpair_send.at[d, n],
@@ -598,20 +604,17 @@
         for d in range(1, nchip):
             which = lax.rem(chip + d, nchip)
             for n in range(npiece):
-                cols = wobuf[depth:, n * cut : (n + 1) * cut]
-                mine[d * npiece + n] = nn(mixed_rows(which, 1 - core), cols).astype(BF16)
-                pair_copy(d, n).start()
+                split(d, n, nn(mixed_rows(which), wobuf[depth:, n * cut : (n + 1) * cut]))
 
     @scoped("ret_send")
     def ret_send():
         for d in range(1, nchip):
-            which = lax.rem(chip + d, nchip)
             for n in range(npiece):
-                cols = wobuf[depth:, n * cut : (n + 1) * cut]
-                part_sum = nn(mixed_rows(which, core), cols)
                 pair_copy(d, n).wait_recv()
-                sent[d * npiece + n] = (part_sum + from_pair[d * npiece + n].astype(F32)).astype(BF16)
-                chip_copy(d, n).start()
+                at = d * npiece + n
+                sent[at] = (kept[at] + from_pair[at].astype(F32)).astype(BF16)
+                if n < npiece - 1:
+                    chip_copy(d, n).start()
 
     def slab_in(d, which):
         index = part(d) * 2 + which
@@ -625,12 +628,6 @@
     for d in range(1, nchip):
         slab_in(d, 0)
         project(d, steps(d)[0])
-        to_later(d, steps(d)[0], 0)
-
-    take_own(0)
-    attend([(tile_of(t, 0), [(base + held[t], part(0))]) for t in range(2)], diagonal=True)
-    take_own_pair(0)
-    own_whole([0], 0)
 
     for d in range(1, nchip):
         slab_in(d, 1)
@@ -644,13 +641,55 @@
         if d == nchip - 1:
             span_state()
         project(d, steps(d)[1])
-        to_later(d, steps(d)[1], 0)
         if d < nchip - 1:
             for step in steps(d):
                 to_later(d, step, 1)
         ret_inner(d)
+    take_own(0)
+    attend([(tile_of(t, 0), [(base + held[t], part(0))]) for t in range(2)], diagonal=True)
+    take_own_pair(0)
+    own_whole([0], 0)
+    pass_states()
+    for d in range(1, nchip):
+        for step in steps(d):
+            to_later(d, step, 0)
     prior_keys([0], 0, True)
-    pass_states()
+
+    lam_copy(1 - core).wait_recv()
+    lam = lamv[head_core, pl.ds(pl.multiple_of(8 * head_no, 8), 8), :][:1, :1]
+
+    def d_copy(t, d):
+        where = {"sp": base + held[t], "tp": part(d) * 2 + head_core}
+        return remote(dsend.at[t, part(d)], dret.at[chip, head_no], ds_sem.at[t, d],
+                      rd_sem.at[chip, head_no], where)
+
+    def d_local(t, d):
+        return pltpu.make_async_copy(dsend.at[t, part(d)], dret.at[chip, head_no],
+                                     rd_sem.at[chip, head_no])
+
+    def home(t, d):
+        return (held[t] == s) & (head_core == core) if d == 0 else False
+
+    @scoped("finish")
+    def finish(t, d):
+        tile = tile_of(t, d)
+        scale = 1.0 / jnp.sum(den[tile], axis=0, keepdims=True)
+        out = acc[tile] * scale
+        merged = out[:, :chunk] - lam * out[:, chunk:]
+        square = jnp.mean(merged * merged, axis=0, keepdims=True)
+        normed = (merged * lax.rsqrt(square + HEAD_EPS)).T
+        dsend[t, part(d)] = (normed * gain_ref[...] * DIFF_SCALE).astype(BF16)
+        if d:
+            d_copy(t, d).start()
+        else:
+
+            @pl.when(home(t, d))
+            def _():
+                d_local(t, d).start()
+
+            @pl.when(jnp.logical_not(home(t, d)))
+            def _():
+                d_copy(t, d).start()
 
     for d in range(1, nchip):
         take_own(d)
@@ -671,47 +710,20 @@
         attend([(tile_of(t, d), [(base + held[t], part(d))]) for t in range(2)], diagonal=True)
         take_own_pair(d)
         own_whole(list(range(d + 1)), d)
-        prior_keys(list(range(d + 1)), d, True)
-
-    lam_copy(1 - core).wait_recv()
-    lam = lamv[head_core, pl.ds(pl.multiple_of(8 * head_no, 8), 8), :][:1, :1]
-
-    def d_copy(t, d):
-        where = {"sp": base + held[t], "tp": part(d) * 2 + head_core}
-        return remote(dsend.at[t, part(d)], dret.at[chip, head_no], ds_sem.at[t, d],
-                      rd_sem.at[chip, head_no], where)
-
-    def d_local(t, d):
-        return pltpu.make_async_copy(dsend.at[t, part(d)], dret.at[chip, head_no],
-                                     rd_sem.at[chip, head_no])
-
-    def home(t, d):
-        return (held[t] == s) & (head_core == core) if d == 0 else False
-
-    @scoped("finish")
-    def finish(t, d):
-        tile = tile_of(t, d)
-        scale = 1.0 / jnp.sum(den[tile], axis=0, keepdims=True)
-        out = acc[tile] * scale
-        merged = out[:, :chunk] - lam * out[:, chunk:]
-        square = jnp.mean(merged * merged, axis=0, keepdims=True)
-        normed = (merged * lax.rsqrt(square + HEAD_EPS)).T
-        dsend[t, part(d)] = (normed * gain_ref[...] * DIFF_SCALE).astype(BF16)
-        if d:
-            d_copy(t, d).start()
-        else:
-
-            @pl.when(home(t, d))
-            def _():
-                d_local(t, d).start()
-
-            @pl.when(jnp.logical_not(home(t, d)))
-            def _():
-                d_copy(t, d).start()
-
-    for d in list(range(1, nchip)) + [0]:
+        if d < nchip - 1:
+            prior_keys(list(range(d + 1)), d, True)
+
+    last = nchip - 1
+    prior_keys(list(range(1, nchip)), last, True)
+    for d in range(1, nchip):
         for t in range(2):
             finish(t, d)
+    for d in range(1, nchip):
+        chip_copy(d, npiece - 1).start()
+    prior_keys([0], last, False)
+    for t in range(2):
+        finish(t, 0)
+
 
     for d in range(1, nchip):
         for n in range(2):
@@ -736,31 +748,32 @@
                     with jax.named_scope("d_wait"):
                         arrival.wait_recv()
 
-    def partial(half, n):
-        inner = pl.ds(pl.multiple_of(half * own_rows, own_rows), own_rows)
+    def partial(n):
         total = nn(
-            jnp.concatenate([dret[chip, h, inner, :] for h in range(heads)] + [mixed_rows(chip, half)], axis=1),
+            jnp.concatenate([dret[chip, h] for h in range(heads)] + [mixed_rows(chip)], axis=1),
             wobuf[:, n * cut : (n + 1) * cut])
         for d in range(1, nchip):
             source = lax.rem(chip + d, nchip)
             total = total + nn(
-                jnp.concatenate([dret[source, h, inner, :] for h in range(heads)], axis=1),
+                jnp.concatenate([dret[source, h] for h in range(heads)], axis=1),
                 wx[d - 1, :, n * cut : (n + 1) * cut])
         return total
 
+    def put(n):
+        return pltpu.make_async_copy(outv.at[n], out_ref.at[:, n * cut : (n + 1) * cut], osem.at[n])
+
     for n in range(npiece):
-        mine[n] = partial(1 - core, n).astype(BF16)
-        pair_copy(0, n).start()
+        split(0, n, partial(n))
     for n in range(npiece):
-        total = partial(core, n)
         with jax.named_scope("p_wait"):
             pair_copy(0, n).wait_recv()
-        total = total + from_pair[n].astype(F32)
+        total = kept[n] + from_pair[n].astype(F32)
         for d in range(1, nchip):
             with jax.named_scope("c_wait"):
                 chip_copy(d, n).wait_recv()
             total = total + from_chip[d * npiece + n].astype(F32)
-        out_ref[:, n * cut : (n + 1) * cut] = total.astype(BF16)
+        outv[n] = total.astype(BF16)
+        put(n).start()
 
     with jax.named_scope("s_wait"):
         for copy in copies:
@@ -827,6 +840,8 @@
             pair_copy(d, n).wait_send()
             if d:
                 chip_copy(d, n).wait_send()
+    for n in range(npiece):
+        put(n).wait()
 
 
 VMEM = pl.BlockSpec(memory_space=pltpu.VMEM)
@@ -861,7 +876,7 @@
         functools.partial(layer_kernel, nsp, ntp, widths, heads, rheads),
         out_shape=jax.ShapeDtypeStruct((own_rows, width), BF16),
         in_specs=[SMEM] + [VMEM] * 5 + [ANY] * (len(weights) + 2),
-        out_specs=VMEM,
+        out_specs=ANY,
         scratch_shapes=[
             pltpu.VMEM((ntp, own_rows, model), BF16),
             pltpu.VMEM((model, sum(widths)), BF16),
@@ -889,6 +904,8 @@
             pltpu.VMEM((nchip * npiece, own_rows, cut), BF16),
             pltpu.VMEM((nchip * npiece, own_rows, cut), BF16),
             pltpu.VMEM((nchip * npiece, own_rows, cut), BF16),
+            pltpu.VMEM((nchip * npiece, own_rows, cut), F32),
+            pltpu.VMEM((npiece, own_rows, cut), BF16),
             DMA((len(weights) + 2,)),
             DMA((2,)),
             DMA((nchip, 2)),
@@ -913,6 +930,7 @@
             DMA((nchip, npiece)),
             DMA((nchip, npiece)),
             DMA((nchip, npiece)),
+            DMA((npiece,)),
         ],
         compiler_params=params(0),
         name="layer",

time: 57 us -> 53.8 us (0.944)
  Pallas kernels: 55 us -> 51.8 us
    pallas_call x1, Pallas kernels: 55 us -> 51.8 us  [on_device(): pl.pallas_call(functools.partial(layer_kernel, nsp, ntp, widths, heads, r...]
where the time goes in v3:
time: 53.8 us; the launch traced here: 53.6 us
  Pallas kernels  51.8 us (96%)
  local copies, waits for them, and re-layouts  1.88 us (3%)
    pallas_call x1, Pallas kernels, on_device(): pl.pallas_call(functools.partial(layer_kernel, nsp, ntp, widths, heads, r...  51.8 us
    unnamed x1, local copies, waits for them, and re-layouts  1.88 us

profile of v3, /device:TPU:17, one launch (start us, length us, event | category | flops | bytes accessed | tf_op | source)
XLA Modules:
  0.0 53.6 jit_solution(12267280240214820589)
XLA Ops:
  0.0 51.8 %layer.1 = bf16[128,2048]{1,0:T(8,128)(2,1)} custom-call(f32[2]{0:T(128)} %lam_ref.1, bf16[128,2048]{1,0:T(8,128)(2,1)} %tokens_ref.1, f32[1,2048]{1,0:T(1,128)} %bitcast.2, f32[1,128]{1,0:T(1,128)} %bitcast.3, f32[2,512]{1,0:T(2,128)} %log_ref.1, f32[2,64,128]{2,1,0:T(8,128)} %init_ref.1, bf16[2048,128]{1,0:T(8,128)(2,1)} %refs_0_.1, ...), custom_call_target="tpu_custom_call" | custom-call | tf_op jit(solution)/shard_map/layer/pallas_call | solution.py:875
  51.8 1.9 %copy.18 = bf16[128,2048]{1,0:T(8,128)(2,1)} copy(bf16[128,2048]{1,0:T(8,128)(2,1)} %layer.1) | data formatting | bytes 1048576
